TPU v7x, 32 devices: a whole 2x2x4 slice. The times are simulated.
32 devices in a mesh: sp: 8 (over z, y), tp: 4 (over x, core).
Axes of the slice: x: 2, y: 2, z: 4, core: 2. Of those that a mesh axis runs over, the one named last changes fastest.
Arguments:
- head_queries: bfloat16 [2048, 2048], P('sp', 'tp'), may hold values from -6 to 6
- head_keys: bfloat16 [2048, 2048], P('sp', 'tp'), may hold values from -6 to 6
- head_values: bfloat16 [2048, 2048], P('sp', 'tp'), may hold values from -6 to 6
- decay_logits: bfloat16 [2048, 2048], P('sp', 'tp'), may hold values from -12 to 1
- learning_logits: bfloat16 [2048, 32], P('sp', 'tp'), may hold values from -9 to 2
- surge_decay: float32 [2048, 32], P('sp', 'tp'), may hold values from -0.7 to 0
- documents: int32 [2048], P('sp'), may hold values from 0 to 2, never falling along the last dimension, each value on 1 to 1536 neighbouring positions
- residual: bfloat16 [2048, 2048], P(('sp', 'tp')), may hold values from -6 to 6
- head_norm_scale: float32 [2048], P('tp'), may hold values from 0.1 to 1.9
- mixer_output_weight: bfloat16 [2048, 2048], P('tp'), may hold values from -0.125 to 0.125
- layer_norm_scale: float32 [2048], replicated, may hold values from 0.1 to 1.9
- routes: int32 [2048, 2], P('sp'), may hold values from 0 to 15, all different within a row; in each aligned block of 64 rows (0 to 63, 64 to 127, ...) at most 12 rows name the same one
- routing_weight: float32 [2048, 2], P(('sp', 'tp')), may hold values from 0.3 to 1.5
- routed_gate_weight: bfloat16 [16, 2048, 1024], P('sp', None, 'tp'), may hold values from -0.125 to 0.125
- routed_up_weight: bfloat16 [16, 2048, 1024], P('sp', None, 'tp'), may hold values from -0.125 to 0.125
- routed_down_weight: bfloat16 [16, 1024, 2048], P('sp', 'tp'), may hold values from -0.1875 to 0.1875
- common_gate_weight: bfloat16 [2048, 512], P(None, 'tp'), may hold values from -0.125 to 0.125
- common_up_weight: bfloat16 [2048, 512], P(None, 'tp'), may hold values from -0.125 to 0.125
- common_down_weight: bfloat16 [512, 2048], P('tp'), may hold values from -0.25 to 0.25
Outputs:
- layer_out: bfloat16 [2048, 2048], P(('sp', 'tp'))
Inputs may be any that keep to these rules, and one draw needn't show every extreme that they name: `documents`: numbers never fall along the positions; each document holds 1 to 1536 positions and one holds exactly 1536. `routes`: each row names 2 different experts; in each aligned block of 64 rows no expert is named by more than 12 rows, a bound that some block reaches.
All inputs are finite; a program needn't handle non-finite values.
Results may differ from a plain program's by a relative error of at most 0.019.
Values may be sent and summed in bfloat16 or wider, within the bound.
A program may use at most 128 MiB of HBM per device.

v0:
```python
import jax
import jax.numpy as jnp
from jax import lax
from jax.experimental import pallas as pl
from jax.experimental.pallas import tpu as pltpu
from jax.sharding import PartitionSpec as P

HEAD = 64
EXP_DEV = 2
TOP = 2
BLOCK_SPAN = 64
TOK_DEV = 64


residual_scale = 2.0**0.5
group_eps = 0.00064
norm_eps = 1e-05
unit_eps = 1e-06
highest = lax.Precision.HIGH


MESH = pl.DeviceIdType.MESH
VMEM = pl.BlockSpec(memory_space=pltpu.VMEM)


def remote(src, dst, send_sem, recv_sem, axis, index):
    return pltpu.make_async_remote_copy(
        src_ref=src,
        dst_ref=dst,
        send_sem=send_sem,
        recv_sem=recv_sem,
        device_id={axis: index},
        device_id_type=MESH,
    )


def greet(groups):
    barrier = pltpu.get_barrier_semaphore()
    count = 0
    for axis, size in groups:
        me = lax.axis_index(axis)
        for step in range(1, size):
            pl.semaphore_signal(
                barrier,
                inc=1,
                device_id={axis: lax.rem(me + step, size)},
                device_id_type=MESH,
            )
            count += 1
    pl.semaphore_wait(barrier, count)


def chain_kernel(
    size, maps, adds, first_doc, last_doc, carry, prior_doc, stage, send_sem, recv_sem
):
    me = lax.axis_index("sp")
    following = lax.rem(me + 1, size)
    previous = lax.rem(me + size - 1, size)
    barrier = pltpu.get_barrier_semaphore()
    for neighbour in (following, previous):
        pl.semaphore_signal(
            barrier, inc=1, device_id={"sp": neighbour}, device_id_type=MESH
        )
    pl.semaphore_wait(barrier, 2)

    @pl.when(me == 0)
    def _():
        carry[...] = jnp.zeros_like(carry)
        prior_doc[...] = jnp.zeros_like(prior_doc)

    pieces = maps.shape[0]
    doc_hop = remote(
        last_doc, prior_doc, send_sem.at[pieces], recv_sem.at[pieces], "sp", following
    )

    @pl.when(me < size - 1)
    def _():
        doc_hop.start()

    @pl.when(me > 0)
    def _():
        doc_hop.wait_recv()

    joined = jnp.where(prior_doc[0:1, :] == first_doc[0:1, :], 1.0, 0.0)
    for piece in range(pieces):
        hop = remote(
            stage.at[piece],
            carry.at[piece],
            send_sem.at[piece],
            recv_sem.at[piece],
            "sp",
            following,
        )

        @pl.when(me > 0)
        def _():
            hop.wait_recv()

        @pl.when(me < size - 1)
        def _():
            stage[piece] = (
                jnp.dot(
                    carry[piece].astype(jnp.float32) * joined,
                    maps[piece],
                    preferred_element_type=jnp.float32,
                    precision=lax.Precision.HIGHEST,
                )
                + adds[piece]
            ).astype(stage.dtype)
            hop.start()

    for piece in range(pieces):
        hop = remote(
            stage.at[piece],
            carry.at[piece],
            send_sem.at[piece],
            recv_sem.at[piece],
            "sp",
            following,
        )

        @pl.when(me < size - 1)
        def _():
            hop.wait_send()

    @pl.when(me < size - 1)
    def _():
        doc_hop.wait_send()


def chain_states(maps, adds, first_doc, last_doc):
    size = lax.axis_size("sp")
    pieces = maps.shape[0]
    return pl.pallas_call(
        lambda *refs: chain_kernel(size, *refs),
        out_shape=(
            jax.ShapeDtypeStruct(adds.shape, jnp.bfloat16),
            jax.ShapeDtypeStruct(first_doc.shape, first_doc.dtype),
        ),
        in_specs=[VMEM] * 4,
        out_specs=(VMEM, VMEM),
        scratch_shapes=[
            pltpu.VMEM(adds.shape, jnp.bfloat16),
            pltpu.SemaphoreType.DMA((pieces + 1,)),
            pltpu.SemaphoreType.DMA((pieces + 1,)),
        ],
        compiler_params=pltpu.CompilerParams(collective_id=1, has_side_effects=True),
    )(maps, adds, first_doc, last_doc)


def tp_reduce_kernel(size, groups, sends_back, *refs):
    if sends_back:
        (parts, extra, out, extra_out, near, pair, far, enear, epair, efar, stage) = refs[:11]
        sems = refs[11:]
    else:
        (parts, out, near, pair, far) = refs[:5]
        sems = refs[5:]
    nsend, nrecv, fsend, frecv = sems[:4]
    me = lax.axis_index("tp")
    own = lax.axis_index("sp")
    half = size // 2
    partner = me + 1 - 2 * lax.rem(me, 2)
    pieces = parts.shape[1]
    greet((("tp", size), ("sp", groups)) if sends_back else (("tp", size),))

    jobs = []
    for step in range(pieces):
        where = lax.rem(own + 1 + step, pieces) if sends_back else step
        jobs.append((step, parts, near, pair, far, where))
    if sends_back:
        jobs.append((pieces, extra, enear, epair, efar, 0))

    def near_copy(job, k):
        slot, src, to, _, _, where = job
        return remote(
            src.at[lax.rem(partner + 2 * k, size), where],
            to.at[k, where],
            nsend.at[slot, k],
            nrecv.at[slot, k],
            "tp",
            partner,
        )

    def far_copy(job, k):
        slot, _, _, src, to, where = job
        return remote(
            src.at[k - 1, where],
            to.at[k - 1, where],
            fsend.at[slot, k],
            frecv.at[slot, k],
            "tp",
            lax.rem(me + 2 * k, size),
        )

    for job in jobs:
        for k in range(half - 1, -1, -1):
            near_copy(job, k).start()

    def add_pair(job):
        slot, src, to, mid, _, where = job
        for k in range(1, half):
            near_copy(job, k).wait_recv()
            mid[k - 1, where] = (
                src[lax.rem(me + 2 * k, size), where].astype(jnp.float32)
                + to[k, where].astype(jnp.float32)
            ).astype(jnp.bfloat16)
            far_copy(job, k).start()

    def back_copy(step):
        target = lax.rem(own + 1 + step, pieces)
        return remote(
            stage.at[target], out.at[own], sems[4].at[step], sems[5].at[step], "sp", target
        )

    def finish(job):
        slot, src, to, _, last, where = job
        near_copy(job, 0).wait_recv()
        total = src[me, where].astype(jnp.float32) + to[0, where].astype(jnp.float32)
        for k in range(1, half):
            far_copy(job, k).wait_recv()
            total = total + last[k - 1, where].astype(jnp.float32)
        if not sends_back:
            out[where] = total
        elif slot == pieces:
            extra_out[...] = total
        elif slot == pieces - 1:
            out[own] = total.astype(jnp.bfloat16)
        else:
            stage[where] = total.astype(jnp.bfloat16)
            back_copy(slot).start()

    lag = 2
    for turn in range(len(jobs) + lag):
        if turn < len(jobs):
            add_pair(jobs[turn])
        if turn >= lag:
            finish(jobs[turn - lag])
    for job in jobs:
        for k in range(half):
            near_copy(job, k).wait_send()
        for k in range(1, half):
            far_copy(job, k).wait_send()
    if sends_back:
        for step in range(pieces - 1):
            back_copy(step).wait_send()
            sender = lax.rem(own - 1 - step + pieces, pieces)
            remote(
                stage.at[sender], out.at[sender], sems[4].at[step], sems[5].at[step], "sp", sender
            ).wait_recv()


def tp_reduce(parts):
    size, pieces, rows, width = parts.shape
    half = size // 2
    kind = jnp.bfloat16
    return pl.pallas_call(
        lambda *refs: tp_reduce_kernel(size, 1, False, *refs),
        out_shape=jax.ShapeDtypeStruct((pieces, rows, width), jnp.float32),
        in_specs=[VMEM],
        out_specs=VMEM,
        scratch_shapes=[
            pltpu.VMEM((half, pieces, rows, width), kind),
            pltpu.VMEM((half - 1, pieces, rows, width), kind),
            pltpu.VMEM((half - 1, pieces, rows, width), kind),
        ]
        + [pltpu.SemaphoreType.DMA((pieces, half))] * 4,
        compiler_params=pltpu.CompilerParams(collective_id=2, has_side_effects=True),
    )(parts)


def tp_reduce_return(parts, extra):
    size, pieces, rows, width = parts.shape
    more = extra.shape[1]
    half = size // 2
    kind = jnp.bfloat16
    return pl.pallas_call(
        lambda parts_ref, extra_ref, *refs: tp_reduce_kernel(
            size, pieces, True, parts_ref, extra_ref, *refs
        ),
        out_shape=(
            jax.ShapeDtypeStruct((pieces, rows, width), kind),
            jax.ShapeDtypeStruct((more, width), jnp.float32),
        ),
        in_specs=[VMEM, VMEM],
        out_specs=(VMEM, VMEM),
        scratch_shapes=[
            pltpu.VMEM((half, pieces, rows, width), kind),
            pltpu.VMEM((half - 1, pieces, rows, width), kind),
            pltpu.VMEM((half - 1, pieces, rows, width), kind),
            pltpu.VMEM((half, 1, more, width), kind),
            pltpu.VMEM((half - 1, 1, more, width), kind),
            pltpu.VMEM((half - 1, 1, more, width), kind),
            pltpu.VMEM((pieces, rows, width), kind),
        ]
        + [pltpu.SemaphoreType.DMA((pieces + 1, half))] * 4
        + [pltpu.SemaphoreType.DMA((pieces,))] * 2,
        compiler_params=pltpu.CompilerParams(
            collective_id=3, has_side_effects=True, vmem_limit_bytes=60 * 1024 * 1024
        ),
    )(parts, extra[:, None])


def dispatch_kernel(
    size, groups, outgoing, stream, arrived, rows_all, local, asend, arecv, nsend, nrecv, fsend, frecv, gsend, grecv
):
    me = lax.axis_index("tp")
    own = lax.axis_index("sp")
    half = size // 2
    partner = me + 1 - 2 * lax.rem(me, 2)
    greet((("tp", size), ("sp", groups)))

    def exchange(step):
        return remote(
            outgoing.at[lax.rem(own + step, groups)],
            arrived.at[me, own],
            asend.at[step],
            arecv.at[step],
            "sp",
            lax.rem(own + step, groups),
        )

    def place(step, who):
        if step == groups:
            return rows_all.at[who]
        return arrived.at[who, lax.rem(own - step + groups, groups)]

    def source(step):
        if step == groups:
            return stream
        return outgoing.at[own] if step == 0 else place(step, me)

    def near_copy(step):
        return remote(source(step), place(step, me), nsend.at[step], nrecv.at[step], "tp", partner)

    def far_copy(step, k):
        return remote(
            source(step),
            place(step, me),
            fsend.at[step, k],
            frecv.at[step, k],
            "tp",
            lax.rem(me + 2 * k, size),
        )

    def forward(step, k):
        who = place(step, lax.rem(me - 2 * k + size, size))
        return remote(who, who, gsend.at[step, k], grecv.at[step, k], "tp", partner)

    def start_own(step):
        for k in range(1, half):
            far_copy(step, k).start()
        near_copy(step).start()

    def pass_on(step):
        for k in range(1, half):
            far_copy(step, k).wait_recv()
            forward(step, k).start()

    keep_block = pltpu.make_async_copy(outgoing.at[own], arrived.at[me, own], local.at[0])
    keep_rows = pltpu.make_async_copy(stream, rows_all.at[me], local.at[1])
    for step in range(1, groups):
        exchange(step).start()
    keep_block.start()
    keep_rows.start()
    order = [groups] + list(range(groups))
    for turn, step in enumerate(order):
        if 0 < step < groups:
            exchange(step).wait_recv()
        start_own(step)
        if turn > 0:
            pass_on(order[turn - 1])
    pass_on(order[-1])
    keep_block.wait()
    keep_rows.wait()
    for step in range(1, groups):
        exchange(step).wait_send()
    for step in order:
        near_copy(step).wait()
        for k in range(1, half):
            far_copy(step, k).wait_send()
            forward(step, k).wait()


def dispatch(outgoing, stream):
    size = lax.axis_size("tp")
    groups, rows, width = outgoing.shape
    half = size // 2
    dma = pltpu.SemaphoreType.DMA
    return pl.pallas_call(
        lambda *refs: dispatch_kernel(size, groups, *refs),
        out_shape=(
            jax.ShapeDtypeStruct((size, groups, rows, width), jnp.bfloat16),
            jax.ShapeDtypeStruct((size,) + stream.shape, jnp.bfloat16),
        ),
        in_specs=[VMEM, VMEM],
        out_specs=(VMEM, VMEM),
        scratch_shapes=[dma((2,)), dma((groups,)), dma((groups,))]
        + [dma((groups + 1,))] * 2
        + [dma((groups + 1, half))] * 4,
        compiler_params=pltpu.CompilerParams(collective_id=4, has_side_effects=True),
    )(outgoing, stream)


def pair_scores(left, right):
    return jnp.einsum("bhtn,bhsn->bhts", left, right, precision=highest)


def apply_scores(scores, operand):
    return jnp.einsum("bhts,bhsn->bhtn", scores, operand, precision=highest)


def split_heads(values, block_list, head_number):
    return (
        values.astype(jnp.float32)
        .reshape(block_list, BLOCK_SPAN, head_number, HEAD)
        .transpose(0, 2, 1, 3)
    )


def unit_lower_inverse(strict_part):
    power = strict_part
    inverse = jnp.eye(BLOCK_SPAN, dtype=jnp.float32) - strict_part
    reach = 2
    while reach < BLOCK_SPAN:
        power = apply_scores(power, power)
        inverse = inverse + apply_scores(inverse, power)
        reach = reach * 2
    return inverse


def linear_recurrence_mixer(
    head_queries,
    head_keys,
    head_values,
    decay_logits,
    learning_logits,
    surge_decay,
    documents,
    head_norm_scale,
):
    length, local_width = head_queries.shape
    head_number = local_width // HEAD
    block_list = length // BLOCK_SPAN
    read_heads = split_heads(head_queries, block_list, head_number)
    key_heads = split_heads(head_keys, block_list, head_number)
    values = split_heads(head_values, block_list, head_number)
    unit_keys = key_heads * lax.rsqrt(jnp.sum(key_heads * key_heads, -1, keepdims=True) + unit_eps)
    learn_rate = (
        jax.nn.sigmoid(learning_logits.astype(jnp.float32))
        .reshape(block_list, BLOCK_SPAN, head_number)
        .transpose(0, 2, 1)
    )
    surge_list = surge_decay.reshape(block_list, BLOCK_SPAN, head_number).transpose(0, 2, 1)
    decay_logarithm = split_heads(
        -jnp.exp(-jax.nn.softplus(-decay_logits.astype(jnp.float32)) - 0.5), block_list, head_number
    )
    decay_logarithm = decay_logarithm + surge_list[..., None]
    cumulative = jnp.cumsum(decay_logarithm, axis=2)
    before = cumulative - decay_logarithm
    doc_blocks = documents.reshape(block_list, BLOCK_SPAN)
    prior_doc = jnp.concatenate([doc_blocks[:1, 0], doc_blocks[:-1, -1]])
    joined = (doc_blocks == prior_doc[:, None]).astype(jnp.float32)[:, None, :, None]
    same_doc = doc_blocks[:, :, None] == doc_blocks[:, None, :]
    later_pos = lax.broadcasted_iota(jnp.int32, (BLOCK_SPAN, BLOCK_SPAN), 0)
    earlier_pos = lax.broadcasted_iota(jnp.int32, (BLOCK_SPAN, BLOCK_SPAN), 1)
    strict = (same_doc & (later_pos > earlier_pos)[None]).astype(jnp.float32)[:, None]
    causal_incl = (same_doc & (later_pos >= earlier_pos)[None]).astype(jnp.float32)[:, None]
    ahead_unit = unit_keys * jnp.exp(before)
    back_unit = unit_keys * jnp.exp(-cumulative)
    back_key = key_heads * jnp.exp(-cumulative)
    forward = read_heads * jnp.exp(cumulative)
    lower_part = pair_scores(ahead_unit, back_unit) * strict * learn_rate[:, :, None, :]
    mix_key = pair_scores(ahead_unit, back_key) * strict
    right_side = jnp.concatenate([ahead_unit * joined, apply_scores(mix_key, values)], -1)
    solved = apply_scores(unit_lower_inverse(lower_part), right_side)
    carry_map = solved[..., :HEAD]
    local_pull = solved[..., HEAD:]
    read_unit = pair_scores(forward, back_unit) * causal_incl * -learn_rate[:, :, None, :]
    read_key = pair_scores(forward, back_key) * causal_incl
    local_out = apply_scores(read_unit, local_pull) + apply_scores(read_key, values)
    read_start = forward * joined + apply_scores(read_unit, carry_map)
    block_total = cumulative[:, :, -1:, :]
    tail_mask = (doc_blocks == doc_blocks[:, -1:]).astype(jnp.float32)[:, None, :, None]
    end_unit = unit_keys * jnp.exp(block_total - cumulative) * tail_mask * -learn_rate[..., None]
    end_key = key_heads * jnp.exp(block_total - cumulative) * tail_mask
    block_map = jnp.eye(HEAD, dtype=jnp.float32) * (jnp.exp(block_total) * joined[:, :, -1:, :])
    block_map = block_map + jnp.einsum("bhsn,bhsm->bhnm", carry_map, end_unit, precision=highest)
    block_add = jnp.einsum("bhsv,bhsm->bhvm", local_pull, end_unit, precision=highest)
    block_add = block_add + jnp.einsum("bhsv,bhsm->bhvm", values, end_key, precision=highest)
    identity_map = jnp.broadcast_to(jnp.eye(HEAD, dtype=jnp.float32), (head_number, HEAD, HEAD))
    carried = jnp.zeros((head_number, HEAD, HEAD), jnp.float32)
    through = identity_map
    outputs = []
    starts = []
    for block_index in range(block_list):
        outputs.append(
            local_out[block_index]
            + jnp.einsum("hlm,hvm->hlv", read_start[block_index], carried, precision=highest)
        )
        starts.append(
            jnp.einsum("hlm,hnm->hln", read_start[block_index], through, precision=highest)
        )
        carried = (
            jnp.einsum("hvn,hnm->hvm", carried, block_map[block_index], precision=highest)
            + block_add[block_index]
        )
        through = jnp.einsum("hvn,hnm->hvm", through, block_map[block_index], precision=highest)
    first_doc = jnp.full((8, 2 * HEAD), documents[0].astype(jnp.float32))
    last_doc = jnp.full((8, 2 * HEAD), documents[-1].astype(jnp.float32))
    pairs = head_number // 2
    zero_block = jnp.zeros((pairs, HEAD, HEAD), jnp.float32)
    maps = through.reshape(pairs, 2, HEAD, HEAD)
    maps = jnp.concatenate(
        [
            jnp.concatenate([maps[:, 0], zero_block], -1),
            jnp.concatenate([zero_block, maps[:, 1]], -1),
        ],
        1,
    )
    adds = carried.reshape(pairs, 2, HEAD, HEAD)
    arriving, prior = chain_states(
        maps, jnp.concatenate([adds[:, 0], adds[:, 1]], -1), first_doc, last_doc
    )
    joined_here = (prior[0, 0] == first_doc[0, 0]).astype(jnp.float32)
    incoming = jnp.stack([arriving[..., :HEAD], arriving[..., HEAD:]], 1).reshape(
        head_number, HEAD, HEAD
    )
    incoming = incoming.astype(jnp.float32) * joined_here
    head_read = jnp.stack(outputs) + jnp.einsum(
        "bhln,hvn->bhlv", jnp.stack(starts), incoming, precision=highest
    )
    centre = jnp.mean(head_read, -1, keepdims=True)
    spread = jnp.mean(jnp.square(head_read - centre), -1, keepdims=True)
    normed = (
        ((head_read - centre) * lax.rsqrt(spread + group_eps))
        .transpose(0, 2, 1, 3)
        .reshape(length, local_width)
    )
    return (normed * head_norm_scale).astype(jnp.bfloat16)


def per_device(
    head_queries,
    head_keys,
    head_values,
    decay_logits,
    learning_logits,
    surge_decay,
    documents,
    residual,
    head_norm_scale,
    mixer_output_weight,
    layer_norm_scale,
    routes,
    routing_weight,
    routed_gate_weight,
    routed_up_weight,
    routed_down_weight,
    common_gate_weight,
    common_up_weight,
    common_down_weight,
):
    head_outputs = linear_recurrence_mixer(
        head_queries,
        head_keys,
        head_values,
        decay_logits,
        learning_logits,
        surge_decay,
        documents,
        head_norm_scale,
    )
    quarters = lax.axis_size("tp")
    groups = lax.axis_size("sp")
    own_rows, model_width = residual.shape
    pieces = own_rows // 16
    mixed_parts = jnp.dot(
        head_outputs, mixer_output_weight, preferred_element_type=jnp.float32
    ).astype(jnp.bfloat16)
    mixed_rows = tp_reduce(mixed_parts.reshape(quarters, pieces, 16, model_width)).reshape(
        own_rows, model_width
    )
    summed = residual_scale * residual.astype(jnp.float32) + mixed_rows
    centre = jnp.mean(summed, -1, keepdims=True)
    spread = jnp.mean(jnp.square(summed - centre), -1, keepdims=True)
    stream = ((summed - centre) * lax.rsqrt(spread + norm_eps) * layer_norm_scale).astype(
        jnp.bfloat16
    )
    experts = EXP_DEV * groups
    capacity = max(2, (3 * TOK_DEV * TOP + 2 * experts - 1) // (2 * experts))
    chosen = routes.reshape(quarters, own_rows * TOP)
    onehot = (chosen[..., None] == jnp.arange(experts, dtype=jnp.int32)).astype(jnp.int32)
    ranking = jnp.sum(jnp.cumsum(onehot, 1) * onehot, -1) - 1
    slot_index = chosen * capacity + ranking
    own_slots = lax.dynamic_index_in_dim(slot_index, lax.axis_index("tp"), 0, keepdims=False)
    own_slots = own_slots.reshape(own_rows, TOP)
    slots = jnp.arange(experts * capacity, dtype=jnp.int32)
    hits = own_slots[:, :, None] == slots
    spread_to = jnp.any(hits, 1).astype(jnp.bfloat16)
    block_rows = EXP_DEV * capacity
    outgoing = jnp.einsum(
        "ts,td->sd", spread_to, stream, preferred_element_type=jnp.float32
    ).astype(jnp.bfloat16)
    arrived_all, rows_all = dispatch(outgoing.reshape(groups, block_rows, model_width), stream)
    rows_in = arrived_all.reshape(quarters * groups * block_rows, model_width)
    hosted = (jnp.arange(rows_in.shape[0], dtype=jnp.int32) % block_rows) // capacity
    hidden_list = []
    for expert in range(EXP_DEV):
        gated = jnp.dot(rows_in, routed_gate_weight[expert], preferred_element_type=jnp.float32)
        lifted = jnp.dot(rows_in, routed_up_weight[expert], preferred_element_type=jnp.float32)
        hidden = (jax.nn.silu(gated) * lifted).astype(jnp.bfloat16)
        hidden_list.append(
            jnp.where((hosted == expert)[:, None], hidden, jnp.zeros_like(hidden))
        )
    partial_value = jnp.dot(
        jnp.concatenate(hidden_list, -1),
        routed_down_weight.reshape(-1, model_width),
        preferred_element_type=jnp.float32,
    ).astype(jnp.bfloat16)
    rows_all = rows_all.reshape(quarters * own_rows, model_width)
    shared_gated = jnp.dot(rows_all, common_gate_weight, preferred_element_type=jnp.float32)
    shared_lifted = jnp.dot(rows_all, common_up_weight, preferred_element_type=jnp.float32)
    shared_hidden = (jax.nn.silu(shared_gated) * shared_lifted).astype(jnp.bfloat16)
    shared_part = jnp.dot(
        shared_hidden, common_down_weight, preferred_element_type=jnp.float32
    ).astype(jnp.bfloat16)
    returned, shared_sum = tp_reduce_return(
        partial_value.reshape(quarters, groups, block_rows, model_width),
        shared_part.reshape(quarters, own_rows, model_width),
    )
    weights = jnp.sum(jnp.where(hits, routing_weight[:, :, None], 0.0), 1)
    routed = jnp.dot(
        weights,
        returned.reshape(experts * capacity, model_width).astype(jnp.float32),
        precision=lax.Precision.HIGHEST,
    )
    return (residual_scale * stream.astype(jnp.float32) + routed + shared_sum).astype(jnp.bfloat16)


def solution(mesh):
    placed = (
        P("sp", "tp"),
        P("sp", "tp"),
        P("sp", "tp"),
        P("sp", "tp"),
        P("sp", "tp"),
        P("sp", "tp"),
        P("sp"),
        P(("sp", "tp"), None),
        P("tp"),
        P("tp", None),
        P(),
        P("sp", None),
        P(("sp", "tp"), None),
        P("sp", None, "tp"),
        P("sp", None, "tp"),
        P("sp", "tp", None),
        P(None, "tp"),
        P(None, "tp"),
        P("tp", None),
    )
    return jax.shard_map(
        per_device, mesh=mesh, in_specs=placed, out_specs=P(("sp", "tp"), None), check_vma=False
    )
```

profile of v0, /device:TPU:0, one launch (start us, length us, event | category | flops | bytes accessed | tf_op | source)
XLA Modules:
  0.0 216.5 jit_solution(10644321440722979572)
XLA Ops:
  4.3 2.2 fusion.55
  6.4 2.3 %reshape.223 = f32[4,64,8,64]{3,2,1,0:T(8,128)} reshape(f32[256,512]{1,0:T(8,128)} %fusion.55) | data formatting | bytes 1048576 | tf_op jit(solution)/shard_map/reshape | solution.py:415
  8.8 1.6 bitcast_add_fusion
  11.7 2.0 broadcast_multiply_fusion
  13.8 1.3 fusion.2
  21.1 1.7 convolution_add_fusion.1
  22.8 2.3 %convolution_multiply_fusion.1 = f32[4,8,64,64]{3,2,1,0:T(8,128)} fusion(f32[4,8,64,64]{3,2,1,0:T(8,128)S(1)} %get-tuple-element.18, f32[4,64,64]{2,1,0:T(8,128)S(1)} %get-tuple-element.28, f32[4,64,8,64]{3,2,1,0:T(8,128)S(1)} %copy-done.2, f32[4,8,64,64]{3,1,2,0:T(8,128)S(1)} %fusion.34), kind=kOutput, calls=%fused_computation.19 | convolution fusion | flops 50724864 | bytes 2162688 | tf_op jit(solution)/shard_map/bhtn,bhsn->bhts/dot_general | solution.py:405
  25.0 2.1 reshape.227
  27.1 1.9 fusion.56
  29.1 1.9 fusion.14
  31.0 2.2 reshape.242
  33.2 3.4 %fusion.3 = f32[4,8,64,64]{3,2,1,0:T(8,128)S(1)} fusion(f32[4,8,64]{2,1,0:T(8,128)S(1)} %get-tuple-element.38, f32[4,64,64]{2,1,0:T(8,128)S(1)} %get-tuple-element.27, f32[4,64,8,64]{3,2,1,0:T(8,128)} %copy-done.1, f32[4,8,64,64]{3,1,2,0:T(8,128)S(1)} %fusion.34, f32[4,8,64]{2,1,0:T(8,128)S(1)} %get-tuple-element.37, f32[4,64,8,64]{3,2,1,0:T(8,128)} %reshape.242), kind=kOutput, calls=%fused_computation.23 | convolution fusion | flops 51118080 | bytes 2179072 | tf_op jit(solution)/shard_map/bhtn,bhsn->bhts/dot_general | solution.py:405
  36.6 2.3 %fusion.44 = f32[4,8,64,64]{2,3,1,0:T(8,128)} fusion(f32[4,8,64,64]{3,2,1,0:T(8,128)S(1)} %fusion.3, f32[4,8,64,128]{3,2,1,0:T(8,128)S(1)} %copy-done.5), kind=kOutput, calls=%fused_computation.91 | convolution fusion | flops 50331648 | bytes 2097152 | tf_op jit(solution)/shard_map/bhts,bhsn->bhtn/dot_general | solution.py:409
  38.9 2.4 %convolution_multiply_fusion = f32[4,8,64,64]{3,2,1,0:T(8,128)} fusion(f32[4,64,64]{2,1,0:T(8,128)S(1)} %get-tuple-element.27, f32[4,64,8,64]{3,2,1,0:T(8,128)S(1)} %copy-done.3, f32[4,8,64,64]{3,1,2,0:T(8,128)S(1)} %fusion.34, f32[4,64,8,64]{3,2,1,0:T(8,128)S(1)} %copy-done.8), kind=kOutput, calls=%fused_computation.18 | convolution fusion | flops 50855936 | bytes 2162688 | tf_op jit(solution)/shard_map/bhtn,bhsn->bhts/dot_general | solution.py:405
  41.3 2.1 copy.94
  43.4 2.5 %convolution_add_fusion.9 = f32[4,8,64,64]{2,3,1,0:T(8,128)S(1)} fusion(f32[4,8,64,64]{2,3,1,0:T(8,128)} %fusion.44, f32[4,8,64,64]{3,2,1,0:T(8,128)} %convolution_multiply_fusion, bf16[4,64,8,64]{1,3,2,0:T(8,128)(2,1)} %copy.94), kind=kOutput, calls=%fused_computation.17 | convolution fusion | flops 50462720 | bytes 1835008 | tf_op jit(solution)/shard_map/bhts,bhsn->bhtn/dot_general | solution.py:409
  49.5 2.3 %convolution_bitcast_fusion.1 = f32[4,8,64,64]{3,2,1,0:T(8,128)S(1)} fusion(f32[4,64,8,64]{3,2,1,0:T(8,128)} %copy-done.1, f32[4,8,64,64]{3,1,2,0:T(8,128)S(1)} %fusion.34, bf16[4,64,8,64]{1,3,2,0:T(8,128)(2,1)} %copy.94, f32[4,64]{1,0:T(4,128)S(1)} %get-tuple-element.29, f32[4,8,64]{2,1,0:T(8,128)S(1)} %get-tuple-element.19), kind=kOutput, calls=%fused_computation.25 | convolution fusion | flops 50724864 | bytes 1844224 | tf_op jit(solution)/shard_map/bhsv,bhsm->bhvm/dot_general | solution.py:489
  51.9 2.7 %convolution_add_fusion.6 = f32[4,8,64,64]{3,2,1,0:T(8,128)S(1)} fusion(f32[4,8,64,64]{3,2,1,0:T(8,128)S(1)} %convolution_bitcast_fusion.1, f32[4,8,64,128]{3,2,1,0:T(8,128)S(1)} %copy-done.7, f32[4,64,8,64]{3,2,1,0:T(8,128)S(1)} %copy-done.4, f32[4,8,64,64]{3,1,2,0:T(8,128)S(1)} %fusion.34, f32[4,8,64]{2,1,0:T(8,128)S(1)} %get-tuple-element.38, ...), kind=kOutput, calls=%fused_computation.14 | convolution fusion | flops 51118080 | bytes 3171328 | tf_op jit(solution)/shard_map/bhsv,bhsm->bhvm/dot_general | solution.py:488
  54.6 1.6 convolution_add_fusion.7
  68.2 10.2 %shard_map.181 = (bf16[4,64,128]{2,1,0:T(8,128)(2,1)}, f32[8,128]{1,0:T(8,128)}) custom-call(f32[4,128,128]{2,1,0:T(8,128)} %select_maximum_fusion.refs_0_, f32[4,64,128]{2,1,0:T(8,128)} %pad_maximum_fusion.refs_1_, f32[8,128]{1,0:T(8,128)} %broadcast_in_dim.30.refs_2_, f32[8,128]{1,0:T(8,128)} %broadcast_in_dim.34.refs_3_), custom_call_target="tpu_custom_call" | custom-call | tf_op jit(solution)/shard_map/pallas_call | solution.py:134
  81.3 2.8 %fusion.98 = (f32[4,8,64]{2,1,0:T(8,128)S(1)}, f32[4,8,64,64]{2,3,1,0:T(8,128)S(1)}) fusion(f32[8,64,64,1]{2,1,0,3:T(8,128)S(1)} %bitcast.267, f32[1,8,64,64]{3,2,1,0:T(8,128)S(1)} %convolution_bitcast_fusion.2, f32[1,8,64,64]{3,2,1,0:T(8,128)S(1)} %convolution_bitcast_fusion.3, f32[1,8,64,64]{3,2,1,0:T(8,128)S(1)} %convolution_bitcast_fusion.4, ...), kind=kOutput, calls=%fused_computation.210 | convolution fusion | flops 51378176 | bytes 1712128 | tf_op jit(solution)/shard_map/bhln,hvn->bhlv/dot_general | solution.py:529
  84.5 1.3 copy.105
  85.8 1.5 reshape.231
  87.3 3.3 %convolution_convert_fusion.2 = bf16[256,2048]{1,0:T(8,128)(2,1)} fusion(bf16[512,2048]{1,0:T(8,128)(2,1)} %param.28, f32[256,512]{1,0:T(8,128)S(1)} %reshape.231, f32[512]{0:T(512)S(1)} %copy-done.29), kind=kOutput, calls=%fused_computation.2 | convolution fusion | flops 537657344 | bytes 3672064 | tf_op jit(solution)/shard_map/dot_general | solution.py:577
  90.6 12.1 %shard_map.182 = f32[4,16,2048]{2,1,0:T(8,128)} custom-call(bf16[4,4,16,2048]{3,2,1,0:T(8,128)(2,1)} %bitcast.258), custom_call_target="tpu_custom_call" | custom-call | tf_op jit(solution)/shard_map/pallas_call | solution.py:256
  109.1 52.4 %shard_map.183 = (bf16[4,8,24,2048]{3,2,1,0:T(8,128)(2,1)}, bf16[4,64,2048]{2,1,0:T(8,128)(2,1)}) custom-call(bf16[8,24,2048]{2,1,0:T(8,128)(2,1)} %bitcast.263, bf16[64,2048]{1,0:T(8,128)(2,1)} %copy-done.20), custom_call_target="tpu_custom_call" | custom-call | tf_op jit(solution)/shard_map/pallas_call | solution.py:389
  161.5 1.9 fusion.104
  163.4 3.0 %convolution_convert_fusion.1 = bf16[256,2048]{1,0:T(8,128)(2,1)} fusion(bf16[128,2048]{1,0:T(8,128)(2,1)} %param.37, bf16[256,2048]{1,0:T(8,128)(2,1)S(1)} %bitcast.260, bf16[2048,128]{1,0:T(8,128)(2,1)} %param.36, f32[256,128]{1,0:T(8,128)S(1)} %fusion.104), kind=kOutput, calls=%fused_computation.1 | convolution fusion | flops 269156352 | bytes 3276800 | tf_op jit(solution)/shard_map/dot_general | solution.py:624
  166.3 3.3 %fusion.29 = f32[768,256]{0,1:T(8,128)S(1)} fusion(bf16[768,2048]{1,0:T(8,128)(2,1)} %bitcast.271, bf16[2,2048,256]{2,1,0:T(8,128)(2,1)} %param.32), kind=kOutput, calls=%fused_computation.65 | convolution fusion | flops 805306368 | bytes 4980736 | tf_op jit(solution)/shard_map/dot_general | solution.py:609
  174.0 3.5 %convolution_convert_fusion = bf16[768,2048]{1,0:T(8,128)(2,1)} fusion(bf16[512,2048]{1,0:T(8,128)(2,1)S(1)} %bitcast.256, bf16[768,256]{0,1:T(8,128)(2,1)S(1)} %fusion.11, bf16[768,256]{0,1:T(8,128)(2,1)S(1)} %fusion.12), kind=kOutput, calls=%fused_computation | convolution fusion | flops 1613758464 | bytes 6029312 | tf_op jit(solution)/shard_map/dot_general | solution.py:615
  177.5 36.1 %shard_map.184 = (bf16[8,24,2048]{2,1,0:T(8,128)(2,1)}, f32[64,2048]{1,0:T(8,128)}) custom-call(bf16[4,8,24,2048]{3,2,1,0:T(8,128)(2,1)} %bitcast.262, bf16[4,1,64,2048]{3,2,1,0:T(8,128)(2,1)} %bitcast.261), custom_call_target="tpu_custom_call" | custom-call | tf_op jit(solution)/shard_map/pallas_call | solution.py:276
  213.7 2.5 %fusion.1 = bf16[64,2048]{1,0:T(8,128)(2,1)} fusion(f32[64,2048]{1,0:T(8,128)} %get-tuple-element.16, f32[64,192]{1,0:T(8,128)S(1)} %select_reduce_fusion.1, bf16[192,2048]{1,0:T(8,128)(2,1)} %bitcast.266, bf16[64,2048]{1,0:T(8,128)(2,1)S(1)} %copy-done.21), kind=kOutput, calls=%fused_computation.6 | convolution fusion | flops 302645248 | bytes 1884160 | tf_op jit(solution)/shard_map/dot_general | solution.py:632
  (155 shorter events, 39.1 us)
Async XLA Ops:
  0.0 174.0 %copy-start = (bf16[2,256,2048]{2,1,0:T(8,128)(2,1)S(1)}, bf16[2,256,2048]{2,1,0:T(8,128)(2,1)}, u32[]{:S(2)}) copy-start(bf16[2,256,2048]{2,1,0:T(8,128)(2,1)} %param.34) | copy-start | bytes 6291460
  0.0 4.2 %copy-start.28 = (bf16[256,8]{0,1:T(8,128)(2,1)S(1)}, bf16[256,8]{0,1:T(8,128)(2,1)}, u32[]{:S(2)}) copy-start(bf16[256,8]{0,1:T(8,128)(2,1)} %param.23) | copy-start | bytes 12292
  2.6 6.1 %copy-start.27 = (f32[256,8]{0,1:T(8,128)S(1)}, f32[256,8]{0,1:T(8,128)}, u32[]{:S(2)}) copy-start(f32[256,8]{0,1:T(8,128)} %param.24) | copy-start | bytes 24580
  3.8 5.0 %copy-start.1 = (f32[4,64,8,64]{3,2,1,0:T(8,128)}, f32[4,64,8,64]{3,2,1,0:T(8,128)S(1)}, u32[]{:S(2)}) copy-start(f32[4,64,8,64]{3,2,1,0:T(8,128)S(1)} %reshape.243) | copy-start | bytes 1572868
  8.8 2.4 %copy-start.14 = (f32[4,64,8,64]{3,2,1,0:T(8,128)S(1)}, f32[4,64,8,64]{3,2,1,0:T(8,128)}, u32[]{:S(2)}) copy-start(f32[4,64,8,64]{3,2,1,0:T(8,128)} %reshape.223) | copy-start | bytes 1572868
  27.1 2.0 copy-start.18
  27.1 2.0 copy-start.19
  33.2 3.4 %copy-start.5 = (f32[4,8,64,128]{3,2,1,0:T(8,128)S(1)}, f32[4,8,64,128]{3,2,1,0:T(8,128)}, u32[]{:S(2)}) copy-start(f32[4,8,64,128]{3,2,1,0:T(8,128)} %fusion.14) | copy-start | bytes 3145732
  36.6 2.3 %copy-start.12 = (f32[4,8,64,64]{3,2,1,0:T(8,128)}, f32[4,8,64,64]{3,2,1,0:T(8,128)S(1)}, u32[]{:S(2)}) copy-start(f32[4,8,64,64]{3,2,1,0:T(8,128)S(1)} %fusion.3) | copy-start | bytes 1572868
  36.6 2.3 %copy-start.3 = (f32[4,64,8,64]{3,2,1,0:T(8,128)S(1)}, f32[4,64,8,64]{3,2,1,0:T(8,128)}, u32[]{:S(2)}) copy-start(f32[4,64,8,64]{3,2,1,0:T(8,128)} %copy-done.1) | copy-start | bytes 1572868
  36.6 2.3 %copy-start.8 = (f32[4,64,8,64]{3,2,1,0:T(8,128)S(1)}, f32[4,64,8,64]{3,2,1,0:T(8,128)}, u32[]{:S(2)}) copy-start(f32[4,64,8,64]{3,2,1,0:T(8,128)} %reshape.242) | copy-start | bytes 1572868
  43.4 2.6 %copy-start.6 = (f32[4,8,64,128]{3,2,1,0:T(8,128)S(1)}, f32[4,8,64,128]{3,2,1,0:T(8,128)}, u32[]{:S(2)}) copy-start(f32[4,8,64,128]{3,2,1,0:T(8,128)} %fusion.14) | copy-start | bytes 3145732
  43.4 2.6 %copy-start.9 = (f32[4,64,8,64]{3,2,1,0:T(8,128)S(1)}, f32[4,64,8,64]{3,2,1,0:T(8,128)}, u32[]{:S(2)}) copy-start(f32[4,64,8,64]{3,2,1,0:T(8,128)} %reshape.242) | copy-start | bytes 1572868
  43.4 2.6 %copy-start.13 = (f32[4,8,64,64]{3,2,1,0:T(8,128)S(1)}, f32[4,8,64,64]{3,2,1,0:T(8,128)}, u32[]{:S(2)}) copy-start(f32[4,8,64,64]{3,2,1,0:T(8,128)} %copy-done.12) | copy-start | bytes 1572868
  46.1 3.0 %copy-start.25 = (s32[256]{0:T(256)S(1)}, s32[256]{0:T(256)}, u32[]{:S(2)}) copy-start(s32[256]{0:T(256)} %param.25) | copy-start | bytes 3076
  49.2 2.7 %copy-start.4 = (f32[4,64,8,64]{3,2,1,0:T(8,128)S(1)}, f32[4,64,8,64]{3,2,1,0:T(8,128)}, u32[]{:S(2)}) copy-start(f32[4,64,8,64]{3,2,1,0:T(8,128)} %copy-done.1) | copy-start | bytes 1572868
  49.2 2.7 %copy-start.7 = (f32[4,8,64,128]{3,2,1,0:T(8,128)S(1)}, f32[4,8,64,128]{3,2,1,0:T(8,128)}, u32[]{:S(2)}) copy-start(f32[4,8,64,128]{3,2,1,0:T(8,128)} %fusion.14) | copy-start | bytes 3145732
  54.6 1.9 copy-start.11
  54.6 1.9 copy-start.16
  63.3 18.0 %copy-start.23 = (f32[1,8,64,64]{2,3,1,0:T(8,128)S(1)}, f32[1,8,64,64]{2,3,1,0:T(8,128)}, u32[]{:S(2)}) copy-start(f32[1,8,64,64]{2,3,1,0:T(8,128)} %fusion.10) | copy-start | bytes 393220
  63.3 18.0 %copy-start.24 = (f32[1,8,64,64]{3,2,1,0:T(8,128)S(1)}, f32[1,8,64,64]{3,2,1,0:T(8,128)}, u32[]{:S(2)}) copy-start(f32[1,8,64,64]{3,2,1,0:T(8,128)} %convolution_bitcast_fusion.5) | copy-start | bytes 393220
  84.5 2.8 %copy-start.29 = (f32[512]{0:T(512)S(1)}, f32[512]{0:T(512)}, u32[]{:S(2)}) copy-start(f32[512]{0:T(512)} %param.27) | copy-start | bytes 6148
  87.3 15.5 %copy-start.22 = (bf16[64,2048]{1,0:T(8,128)(2,1)S(1)}, bf16[64,2048]{1,0:T(8,128)(2,1)}, u32[]{:S(2)}) copy-start(bf16[64,2048]{1,0:T(8,128)(2,1)} %param.26) | copy-start | bytes 786436
  90.6 14.7 %copy-start.26 = (f32[2048]{0:T(1024)S(1)}, f32[2048]{0:T(1024)}, u32[]{:S(2)}) copy-start(f32[2048]{0:T(1024)} %param.29) | copy-start | bytes 24580
  90.6 15.9 %copy-start.30 = (s32[256,2]{0,1:T(2,128)S(1)}, s32[256,2]{0,1:T(2,128)}, u32[]{:S(2)}) copy-start(s32[256,2]{0,1:T(2,128)} %param.30) | copy-start | bytes 6148
  106.5 2.6 %copy-start.20 = (bf16[64,2048]{1,0:T(8,128)(2,1)}, bf16[64,2048]{1,0:T(8,128)(2,1)S(1)}, u32[]{:S(2)}) copy-start(bf16[64,2048]{1,0:T(8,128)(2,1)S(1)} %multiply_convert_fusion.refs_1_) | copy-start | bytes 786436
  161.5 1.9 copy-start.17
  166.3 3.4 %copy-start.32 = (bf16[4,8,24,2048]{3,2,1,0:T(8,128)(2,1)S(1)}, bf16[4,8,24,2048]{3,2,1,0:T(8,128)(2,1)}, u32[]{:S(2)}) copy-start(bf16[4,8,24,2048]{3,2,1,0:T(8,128)(2,1)} %get-tuple-element.13) | copy-start | bytes 9437188
  166.3 3.8 %copy-start.34 = (bf16[2,2048,256]{2,1,0:T(8,128)(2,1)S(1)}, bf16[2,2048,256]{2,1,0:T(8,128)(2,1)}, u32[]{:S(2)}) copy-start(bf16[2,2048,256]{2,1,0:T(8,128)(2,1)} %param.33) | copy-start | bytes 6291460
  170.1 1.6 copy-start.33
  177.5 36.1 %copy-start.31 = (f32[64,2]{0,1:T(2,128)S(1)}, f32[64,2]{0,1:T(2,128)}, u32[]{:S(2)}) copy-start(f32[64,2]{0,1:T(2,128)} %param.31) | copy-start | bytes 1540
  177.5 36.2 %copy-start.21 = (bf16[64,2048]{1,0:T(8,128)(2,1)S(1)}, bf16[64,2048]{1,0:T(8,128)(2,1)}, u32[]{:S(2)}) copy-start(bf16[64,2048]{1,0:T(8,128)(2,1)} %copy-done.20) | copy-start | bytes 786436
  (3 other events, 3.2 us)
where the time goes:
time: 220 us; the launch traced here: 216 us
  Pallas kernels  111 us (50%)
  matrix products  66.4 us (30%)
  local copies, waits for them, and re-layouts  21.8 us (10%)
  other arithmetic  14.6 us (7%)
  between operations  2.91 us (1%)
    pallas_call x1, Pallas kernels, dispatch(): pl.pallas_call(lambda *refs: dispatch_kernel(size, groups, *refs), out_sh...  52.4 us
    pallas_call x1, Pallas kernels, tp_reduce_return(): pl.pallas_call(lambda parts_ref, extra_ref, *refs: tp_reduce_kernel(size,...  36.1 us
    dot_general x15, matrix products, apply_scores(): return jnp.einsum('bhts,bhsn->bhtn', scores, operand, precision=highest)  17.2 us
    pallas_call x1, Pallas kernels, tp_reduce(): pl.pallas_call(lambda *refs: tp_reduce_kernel(size, 1, False, *refs), out...  12.1 us
    pallas_call x1, Pallas kernels, chain_states(): pl.pallas_call(lambda *refs: chain_kernel(size, *refs), out_shape=(jax.Sh...  10.2 us
    dot_general x4, matrix products, pair_scores(): return jnp.einsum('bhtn,bhsn->bhts', left, right, precision=highest)  9.36 us
    reshape x3, local copies, waits for them, and re-layouts, split_heads(): return values.astype(jnp.float32).reshape(block_list, BLOCK_SPAN, head_nu...  6.49 us
    dot_general x2, matrix products, per_device(): jnp.dot(rows_in, routed_gate_weight[expert], preferred_element_type=jnp.f...  4.42 us

commit v1 on v0

--- a/solution.py
+++ b/solution.py
@@ -16,7 +16,7 @@
 group_eps = 0.00064
 norm_eps = 1e-05
 unit_eps = 1e-06
-highest = lax.Precision.HIGH
+SCORE_PRECISION = lax.Precision.HIGH
 
 
 MESH = pl.DeviceIdType.MESH
@@ -50,102 +50,490 @@
     pl.semaphore_wait(barrier, count)
 
 
-def chain_kernel(
-    size, maps, adds, first_doc, last_doc, carry, prior_doc, stage, send_sem, recv_sem
+def chunk_iota(rows, cols, dim):
+    return lax.broadcasted_iota(jnp.int32, (rows, cols), dim)
+
+
+def mm(left, right, precision=None):
+    return jnp.dot(left, right, preferred_element_type=jnp.float32, precision=precision)
+
+
+def mm_nt(left, right, precision=None):
+    return lax.dot_general(
+        left,
+        right,
+        (((1,), (1,)), ((), ())),
+        preferred_element_type=jnp.float32,
+        precision=precision,
+    )
+
+
+def mm_tn(left, right, precision=None):
+    return lax.dot_general(
+        left,
+        right,
+        (((0,), (0,)), ((), ())),
+        preferred_element_type=jnp.float32,
+        precision=precision,
+    )
+
+
+def narrow(values):
+    return values.astype(jnp.bfloat16)
+
+
+def split(values):
+    top = narrow(values)
+    return top, narrow(values - top.astype(jnp.float32))
+
+
+def mixer_kernel(
+    size,
+    queries,
+    keys,
+    values,
+    decays,
+    rates,
+    surges,
+    docs,
+    scale,
+    out,
+    unit_s,
+    ahead_s,
+    fwd_s,
+    reads_s,
+    solved_s,
+    map_s,
+    add_s,
+    local_s,
+    starts_s,
+    comp_s,
+    far_s,
+    join_s,
+    doc_out,
+    doc_in,
+    padd_out,
+    padd_in,
+    pmap_out,
+    pmap_in,
+    s_out,
+    s_in,
+    doc_sem,
+    padd_sem,
+    pmap_sem,
+    near_sem,
+    next_sem,
+    s_recv,
 ):
     me = lax.axis_index("sp")
+    span = BLOCK_SPAN
+    rows, width = queries.shape
+    chunks = rows // span
+    lanes = 2 * HEAD
+    pairs = width // lanes
+    heads = rates.shape[1]
+    high = lax.Precision.HIGH
+    barrier = pltpu.get_barrier_semaphore()
+    for step in (1, 2, size - 1, size - 2):
+        pl.semaphore_signal(
+            barrier, inc=1, device_id={"sp": lax.rem(me + step, size)}, device_id_type=MESH
+        )
+
+    same_half = (chunk_iota(lanes, lanes, 0) // HEAD) == (chunk_iota(lanes, lanes, 1) // HEAD)
+    ones_half = same_half.astype(jnp.float32)
+    earlier = lax.rem(chunk_iota(span, lanes, 1), HEAD)
+    later = chunk_iota(span, lanes, 0)
+    unit_pair = (earlier == later).astype(jnp.float32)
+    unit_full = (chunk_iota(lanes, lanes, 0) == chunk_iota(lanes, lanes, 1)).astype(jnp.float32)
+
+    def wide(block):
+        return jnp.where(same_half, jnp.concatenate([block, block], 0), 0.0)
+
+    row_docs = docs[...].astype(jnp.float32)
+    row_square = jnp.broadcast_to(row_docs, (rows, rows))
+    diag = chunk_iota(rows, rows, 0) == chunk_iota(rows, rows, 1)
+    doc_col = mm(
+        narrow(jnp.where(diag, row_square, 0.0)), jnp.ones((rows, lanes), jnp.bfloat16)
+    )
+    pick = (
+        lax.rem(chunk_iota(rows, lanes, 0), span) == lax.rem(chunk_iota(rows, lanes, 1), HEAD)
+    ).astype(jnp.bfloat16)
+    wide_rows = 8 * ((chunks + 7) // 8)
+    in_chunk = (chunk_iota(wide_rows, rows, 1) // span) == chunk_iota(wide_rows, rows, 0)
+    doc_row = mm(
+        narrow(jnp.where(in_chunk, jnp.broadcast_to(row_docs, (wide_rows, rows)), 0.0)), pick
+    )
+    same_chunk = (chunk_iota(rows, rows, 0) // span) == (chunk_iota(rows, rows, 1) // span)
+    tri = (
+        (chunk_iota(rows, rows, 0) >= chunk_iota(rows, rows, 1)) & same_chunk
+    ).astype(jnp.bfloat16)
+
+    strict, causal, joined, tail = [], [], [], []
+    for c in range(chunks):
+        col = doc_col[c * span : (c + 1) * span]
+        same_doc = col == doc_row[c : c + 1]
+        strict.append(same_doc & (later > earlier))
+        causal.append(same_doc & (later >= earlier))
+        before_row = doc_col[max(c * span - 1, 0) : max(c * span - 1, 0) + 1]
+        joined.append((col == before_row).astype(jnp.float32))
+        tail.append((col == doc_col[(c + 1) * span - 1 : (c + 1) * span]).astype(jnp.float32))
+
+    doc_out[...] = jnp.broadcast_to(doc_col[rows - 1 : rows], doc_out.shape)
+    pl.semaphore_wait(barrier, 4)
     following = lax.rem(me + 1, size)
-    previous = lax.rem(me + size - 1, size)
-    barrier = pltpu.get_barrier_semaphore()
-    for neighbour in (following, previous):
-        pl.semaphore_signal(
-            barrier, inc=1, device_id={"sp": neighbour}, device_id_type=MESH
-        )
-    pl.semaphore_wait(barrier, 2)
-
-    @pl.when(me == 0)
-    def _():
-        carry[...] = jnp.zeros_like(carry)
-        prior_doc[...] = jnp.zeros_like(prior_doc)
-
-    pieces = maps.shape[0]
-    doc_hop = remote(
-        last_doc, prior_doc, send_sem.at[pieces], recv_sem.at[pieces], "sp", following
-    )
+    doc_hop = remote(doc_out, doc_in, doc_sem.at[0], doc_sem.at[1], "sp", following)
 
     @pl.when(me < size - 1)
     def _():
         doc_hop.start()
 
+    rate_all = jax.nn.sigmoid(rates[...].astype(jnp.float32))
+    surge_all = surges[...]
+
+    def local_pairs(turn, carry):
+        streams = []
+        for half in range(2):
+            p = turn * 2 + half
+            cols = pl.ds(pl.multiple_of(p * lanes, lanes), lanes)
+            spread_heads = (
+                chunk_iota(heads, lanes, 0) == 2 * p + chunk_iota(heads, lanes, 1) // HEAD
+            ).astype(jnp.float32)
+            key = keys[:, cols].astype(jnp.float32)
+            norm = mm(key * key, ones_half, high)
+            unit = key * lax.rsqrt(norm + unit_eps)
+            rate = mm(rate_all, spread_heads, high)
+            surge = mm(surge_all, spread_heads, high)
+            logit = decays[:, cols].astype(jnp.float32)
+            decay = surge - jnp.exp(-0.5) / (1.0 + jnp.exp(-logit))
+            top, rest = split(decay)
+            cumulative = mm(tri, top) + mm(tri, rest)
+            grown = jnp.exp(cumulative)
+            shrunk = jnp.exp(-cumulative)
+            ahead = unit * jnp.exp(cumulative - decay)
+            unit_rate = unit * rate
+            back_unit = unit_rate * shrunk
+            back_key = key * shrunk
+            forward = queries[:, cols].astype(jnp.float32) * grown
+            ahead_s[:, cols] = ahead
+            fwd_s[:, cols] = forward
+            for c in range(chunks):
+                part = slice(c * span, (c + 1) * span)
+                total = cumulative[(c + 1) * span - 1 : (c + 1) * span]
+                ending = jnp.exp(total - cumulative[part]) * tail[c]
+                streams.append(
+                    dict(
+                        c=c,
+                        p=p,
+                        cols=cols,
+                        ahead=ahead[part],
+                        fwd=forward[part],
+                        bu=back_unit[part],
+                        bk=back_key[part],
+                        eu=-unit_rate[part] * ending,
+                        ek=key[part] * ending,
+                        val=values[part, cols].astype(jnp.float32),
+                        keep=jnp.exp(total) * joined[c][span - 1 : span],
+                    )
+                )
+        for s in streams:
+            c = s["c"]
+            scores = mm_nt(
+                jnp.concatenate([s["ahead"], s["fwd"]], 0),
+                jnp.concatenate([wide(s["bu"]), wide(s["bk"])], 0),
+                SCORE_PRECISION,
+            )
+            s["low"] = jnp.where(strict[c], scores[:span, :lanes], 0.0)
+            s["mixk"] = jnp.where(strict[c], scores[:span, lanes:], 0.0)
+            reads_s[c, s["p"], :, :lanes] = narrow(
+                jnp.where(causal[c], -scores[span:, :lanes], 0.0)
+            )
+            reads_s[c, s["p"], :, lanes:] = narrow(jnp.where(causal[c], scores[span:, lanes:], 0.0))
+        base = 16
+        near_block = (earlier // base) == (later // base)
+        for s in streams:
+            s["low_near"] = jnp.where(near_block, s["low"], 0.0)
+            s["inv"] = unit_pair - s["low_near"]
+        for s in streams:
+            s["power"] = mm(s["low_near"], wide(s["low_near"]), high)
+            s["mv"] = mm(s["mixk"], wide(s["val"]))
+        reach = 2
+        while reach < base:
+            last = reach * 2 >= base
+            for s in streams:
+                right = wide(s["power"])
+                if last:
+                    s["inv"] = s["inv"] + mm(s["inv"], right, high)
+                else:
+                    both = mm(jnp.concatenate([s["power"], s["inv"]], 0), right, high)
+                    s["power"] = both[:span]
+                    s["inv"] = s["inv"] + both[span:]
+            reach = reach * 2
+        while base < span:
+            off = ((earlier // base) != (later // base)) & (
+                (earlier // (2 * base)) == (later // (2 * base))
+            )
+            for s in streams:
+                s["mid"] = mm(s["inv"], wide(jnp.where(off, s["low"], 0.0)), high)
+            for s in streams:
+                s["inv"] = s["inv"] - mm(s["mid"], wide(s["inv"]), high)
+            base = base * 2
+        for s in streams:
+            c = s["c"]
+            s["solved"] = mm(
+                s["inv"],
+                jnp.concatenate([wide(s["ahead"] * joined[c]), wide(s["mv"])], 1),
+                high,
+            )
+            solved_s[c, s["p"]] = narrow(s["solved"])
+        for s in streams:
+            c, p = s["c"], s["p"]
+            pull = mm_tn(s["solved"][:, :lanes], s["eu"], high)
+            map_s[c, p] = jnp.where(same_half, pull, 0.0) + unit_full * s["keep"]
+            grown = mm_tn(
+                jnp.concatenate([s["solved"][:, lanes:], s["val"]], 0),
+                jnp.concatenate([s["eu"], s["ek"]], 0),
+                high,
+            )
+            grown = jnp.where(same_half, grown, 0.0)
+            add_s[c, p] = grown[:HEAD] + grown[HEAD:]
+        return carry
+
+    lax.fori_loop(0, pairs // 2, local_pairs, 0)
+
+    state = [None] * pairs
+    for p in range(pairs):
+        state[p] = jnp.concatenate([add_s[0, p], map_s[0, p][:HEAD] + map_s[0, p][HEAD:]], 0)
+    kept = [state]
+    for c in range(1, chunks):
+        state = [
+            mm(kept[-1][p], map_s[c, p], high)
+            + jnp.concatenate([add_s[c, p], jnp.zeros((HEAD, lanes), jnp.float32)], 0)
+            for p in range(pairs)
+        ]
+        kept.append(state)
+    finals = kept[-1]
+
+    @pl.when(me == 0)
+    def _():
+        join_s[...] = jnp.zeros_like(join_s)
+        s_in[...] = jnp.zeros_like(s_in)
+
     @pl.when(me > 0)
     def _():
         doc_hop.wait_recv()
-
-    joined = jnp.where(prior_doc[0:1, :] == first_doc[0:1, :], 1.0, 0.0)
-    for piece in range(pieces):
-        hop = remote(
-            stage.at[piece],
-            carry.at[piece],
-            send_sem.at[piece],
-            recv_sem.at[piece],
+        join_s[...] = (doc_in[...] == doc_col[0:1]).astype(jnp.float32)
+
+    join = join_s[0:1]
+    for p in range(pairs):
+        comp_s[p] = jnp.concatenate([finals[p][:HEAD], finals[p][HEAD:] * join], 0)
+    even = lax.rem(me, 2) == 0
+
+    def pair_hop(p):
+        return (
+            remote(padd_out.at[p], padd_in.at[p], padd_sem.at[0, p], padd_sem.at[1, p], "sp", following),
+            remote(pmap_out.at[p], pmap_in.at[p], pmap_sem.at[0, p], pmap_sem.at[1, p], "sp", following),
+        )
+
+    def state_hop(p, near):
+        sem = near_sem if near else next_sem
+        return remote(
+            s_out.at[p],
+            s_in.at[p],
+            sem.at[p],
+            s_recv.at[p],
             "sp",
-            following,
+            lax.rem(me + (2 if near else 1), size),
         )
 
+    @pl.when(even)
+    def _():
+        for p in range(pairs):
+            padd_out[p] = narrow(comp_s[p, :HEAD])
+            pmap_out[p] = comp_s[p, HEAD:]
+        for p in range(pairs):
+            pair_hop(p)[0].start()
+        for p in range(pairs):
+            pair_hop(p)[1].start()
+
+    def finish_local():
+        for p in range(pairs):
+            cols = slice(p * lanes, (p + 1) * lanes)
+            for c in range(chunks):
+                part = slice(c * span, (c + 1) * span)
+                read_unit = reads_s[c, p, :, :lanes]
+                solved = solved_s[c, p].astype(jnp.float32)
+                local = mm(
+                    reads_s[c, p],
+                    jnp.concatenate(
+                        [
+                            narrow(wide(solved[:, lanes:])),
+                            narrow(wide(values[part, cols].astype(jnp.float32))),
+                        ],
+                        0,
+                    ),
+                )
+                start = fwd_s[part, cols] * joined[c] + mm(
+                    read_unit, narrow(wide(solved[:, :lanes]))
+                )
+                if c > 0:
+                    seen = mm_nt(
+                        narrow(start),
+                        jnp.concatenate(
+                            [
+                                narrow(wide(kept[c - 1][p][:HEAD])),
+                                narrow(wide(kept[c - 1][p][HEAD:])),
+                            ],
+                            0,
+                        ),
+                    )
+                    local = local + seen[:, :lanes]
+                    start = seen[:, lanes:]
+                local_s[part, cols] = local
+                starts_s[part, cols] = narrow(start)
+
+    finish_local()
+
+    @pl.when(jnp.logical_not(even))
+    def _():
+        for p in range(pairs):
+            pair_hop(p)[0].wait_recv()
+            first = padd_in[p]
+            top, rest = split(wide(comp_s[p, HEAD:]))
+            far_s[p, :HEAD] = (
+                mm(jnp.concatenate([first, first], 1), jnp.concatenate([top, rest], 0))
+                + comp_s[p, :HEAD]
+            )
+
+        @pl.when(me == 1)
+        def _():
+            s_in[...] = jnp.zeros_like(s_in)
+            for p in range(pairs):
+                s_out[p] = narrow(far_s[p, :HEAD])
+                state_hop(p, True).start()
+
+        for p in range(pairs):
+            pair_hop(p)[1].wait_recv()
+
+        @pl.when(me > 1)
+        def _():
+            for p in range(pairs):
+                both = mm(pmap_in[p], wide(comp_s[p, HEAD:]), high)
+                far_s[p, HEAD:] = both
+            weights = []
+            for p in range(pairs):
+                top, rest = split(wide(far_s[p, HEAD:]))
+                weights.append(jnp.concatenate([top, rest], 0))
+            for p in range(pairs):
+                state_hop(p, True).wait_recv()
+
+                @pl.when(me < size - 1)
+                def _():
+                    arrived = s_in[p]
+                    s_out[p] = narrow(
+                        mm(jnp.concatenate([arrived, arrived], 1), weights[p]) + far_s[p, :HEAD]
+                    )
+                    state_hop(p, True).start()
+
+        @pl.when(me < size - 1)
+        def _():
+            for p in range(pairs):
+                state_hop(p, False).start()
+
+        for p in range(pairs):
+            top, rest = split(wide(pmap_in[p]))
+            arrived = s_in[p]
+            comp_s[p, :HEAD] = (
+                mm(jnp.concatenate([arrived, arrived], 1), jnp.concatenate([top, rest], 0))
+                + padd_in[p].astype(jnp.float32)
+            )
+
+    @pl.when(even)
+    def _():
         @pl.when(me > 0)
         def _():
-            hop.wait_recv()
-
-        @pl.when(me < size - 1)
-        def _():
-            stage[piece] = (
-                jnp.dot(
-                    carry[piece].astype(jnp.float32) * joined,
-                    maps[piece],
-                    preferred_element_type=jnp.float32,
-                    precision=lax.Precision.HIGHEST,
-                )
-                + adds[piece]
-            ).astype(stage.dtype)
-            hop.start()
-
-    for piece in range(pieces):
-        hop = remote(
-            stage.at[piece],
-            carry.at[piece],
-            send_sem.at[piece],
-            recv_sem.at[piece],
-            "sp",
-            following,
-        )
-
-        @pl.when(me < size - 1)
-        def _():
-            hop.wait_send()
+            for p in range(pairs):
+                state_hop(p, False).wait_recv()
+
+        for p in range(pairs):
+            comp_s[p, :HEAD] = s_in[p].astype(jnp.float32)
+
+    for p in range(pairs):
+        cols = slice(p * lanes, (p + 1) * lanes)
+        incoming = narrow(wide(comp_s[p, :HEAD] * join))
+        read = local_s[:, cols] + mm_nt(starts_s[:, cols], incoming)
+        centred = read - mm(read, ones_half, high) * (1.0 / HEAD)
+        spread = mm(centred * centred, ones_half, high) * (1.0 / HEAD)
+        out[:, cols] = narrow(centred * lax.rsqrt(spread + group_eps) * scale[:, cols])
 
     @pl.when(me < size - 1)
     def _():
         doc_hop.wait_send()
 
-
-def chain_states(maps, adds, first_doc, last_doc):
+    @pl.when(even)
+    def _():
+        for p in range(pairs):
+            for hop in pair_hop(p):
+                hop.wait_send()
+
+    @pl.when(jnp.logical_not(even) & (me < size - 1))
+    def _():
+        for p in range(pairs):
+            state_hop(p, True).wait_send()
+            state_hop(p, False).wait_send()
+
+
+def mixer(queries, keys, values, decays, rates, surges, documents, scale):
     size = lax.axis_size("sp")
-    pieces = maps.shape[0]
+    rows, width = queries.shape
+    lanes = 2 * HEAD
+    pairs = width // lanes
+    chunks = rows // BLOCK_SPAN
+    f32, b16 = jnp.float32, jnp.bfloat16
+    dma = pltpu.SemaphoreType.DMA
     return pl.pallas_call(
-        lambda *refs: chain_kernel(size, *refs),
-        out_shape=(
-            jax.ShapeDtypeStruct(adds.shape, jnp.bfloat16),
-            jax.ShapeDtypeStruct(first_doc.shape, first_doc.dtype),
-        ),
-        in_specs=[VMEM] * 4,
-        out_specs=(VMEM, VMEM),
+        lambda *refs: mixer_kernel(size, *refs),
+        out_shape=jax.ShapeDtypeStruct((rows, width), b16),
+        in_specs=[VMEM] * 8,
+        out_specs=VMEM,
         scratch_shapes=[
-            pltpu.VMEM(adds.shape, jnp.bfloat16),
-            pltpu.SemaphoreType.DMA((pieces + 1,)),
-            pltpu.SemaphoreType.DMA((pieces + 1,)),
+            pltpu.VMEM((8, lanes), f32),
+            pltpu.VMEM((rows, width), f32),
+            pltpu.VMEM((rows, width), f32),
+            pltpu.VMEM((chunks, pairs, BLOCK_SPAN, 2 * lanes), b16),
+            pltpu.VMEM((chunks, pairs, BLOCK_SPAN, 2 * lanes), b16),
+            pltpu.VMEM((chunks, pairs, lanes, lanes), f32),
+            pltpu.VMEM((chunks, pairs, HEAD, lanes), f32),
+            pltpu.VMEM((rows, width), f32),
+            pltpu.VMEM((rows, width), b16),
+            pltpu.VMEM((pairs, lanes, lanes), f32),
+            pltpu.VMEM((pairs, lanes, lanes), f32),
+            pltpu.VMEM((8, lanes), f32),
+            pltpu.VMEM((8, lanes), f32),
+            pltpu.VMEM((8, lanes), f32),
+            pltpu.VMEM((pairs, HEAD, lanes), b16),
+            pltpu.VMEM((pairs, HEAD, lanes), b16),
+            pltpu.VMEM((pairs, HEAD, lanes), f32),
+            pltpu.VMEM((pairs, HEAD, lanes), f32),
+            pltpu.VMEM((pairs, HEAD, lanes), b16),
+            pltpu.VMEM((pairs, HEAD, lanes), b16),
+            dma((2,)),
+            dma((2, pairs)),
+            dma((2, pairs)),
+            dma((pairs,)),
+            dma((pairs,)),
+            dma((pairs,)),
         ],
         compiler_params=pltpu.CompilerParams(collective_id=1, has_side_effects=True),
-    )(maps, adds, first_doc, last_doc)
+    )(
+        queries,
+        keys,
+        values,
+        decays,
+        rates,
+        surges,
+        documents.reshape(1, rows),
+        scale.reshape(1, width),
+    )
 
 
 def tp_reduce_kernel(size, groups, sends_back, *refs):
@@ -401,144 +789,6 @@
     )(outgoing, stream)
 
 
-def pair_scores(left, right):
-    return jnp.einsum("bhtn,bhsn->bhts", left, right, precision=highest)
-
-
-def apply_scores(scores, operand):
-    return jnp.einsum("bhts,bhsn->bhtn", scores, operand, precision=highest)
-
-
-def split_heads(values, block_list, head_number):
-    return (
-        values.astype(jnp.float32)
-        .reshape(block_list, BLOCK_SPAN, head_number, HEAD)
-        .transpose(0, 2, 1, 3)
-    )
-
-
-def unit_lower_inverse(strict_part):
-    power = strict_part
-    inverse = jnp.eye(BLOCK_SPAN, dtype=jnp.float32) - strict_part
-    reach = 2
-    while reach < BLOCK_SPAN:
-        power = apply_scores(power, power)
-        inverse = inverse + apply_scores(inverse, power)
-        reach = reach * 2
-    return inverse
-
-
-def linear_recurrence_mixer(
-    head_queries,
-    head_keys,
-    head_values,
-    decay_logits,
-    learning_logits,
-    surge_decay,
-    documents,
-    head_norm_scale,
-):
-    length, local_width = head_queries.shape
-    head_number = local_width // HEAD
-    block_list = length // BLOCK_SPAN
-    read_heads = split_heads(head_queries, block_list, head_number)
-    key_heads = split_heads(head_keys, block_list, head_number)
-    values = split_heads(head_values, block_list, head_number)
-    unit_keys = key_heads * lax.rsqrt(jnp.sum(key_heads * key_heads, -1, keepdims=True) + unit_eps)
-    learn_rate = (
-        jax.nn.sigmoid(learning_logits.astype(jnp.float32))
-        .reshape(block_list, BLOCK_SPAN, head_number)
-        .transpose(0, 2, 1)
-    )
-    surge_list = surge_decay.reshape(block_list, BLOCK_SPAN, head_number).transpose(0, 2, 1)
-    decay_logarithm = split_heads(
-        -jnp.exp(-jax.nn.softplus(-decay_logits.astype(jnp.float32)) - 0.5), block_list, head_number
-    )
-    decay_logarithm = decay_logarithm + surge_list[..., None]
-    cumulative = jnp.cumsum(decay_logarithm, axis=2)
-    before = cumulative - decay_logarithm
-    doc_blocks = documents.reshape(block_list, BLOCK_SPAN)
-    prior_doc = jnp.concatenate([doc_blocks[:1, 0], doc_blocks[:-1, -1]])
-    joined = (doc_blocks == prior_doc[:, None]).astype(jnp.float32)[:, None, :, None]
-    same_doc = doc_blocks[:, :, None] == doc_blocks[:, None, :]
-    later_pos = lax.broadcasted_iota(jnp.int32, (BLOCK_SPAN, BLOCK_SPAN), 0)
-    earlier_pos = lax.broadcasted_iota(jnp.int32, (BLOCK_SPAN, BLOCK_SPAN), 1)
-    strict = (same_doc & (later_pos > earlier_pos)[None]).astype(jnp.float32)[:, None]
-    causal_incl = (same_doc & (later_pos >= earlier_pos)[None]).astype(jnp.float32)[:, None]
-    ahead_unit = unit_keys * jnp.exp(before)
-    back_unit = unit_keys * jnp.exp(-cumulative)
-    back_key = key_heads * jnp.exp(-cumulative)
-    forward = read_heads * jnp.exp(cumulative)
-    lower_part = pair_scores(ahead_unit, back_unit) * strict * learn_rate[:, :, None, :]
-    mix_key = pair_scores(ahead_unit, back_key) * strict
-    right_side = jnp.concatenate([ahead_unit * joined, apply_scores(mix_key, values)], -1)
-    solved = apply_scores(unit_lower_inverse(lower_part), right_side)
-    carry_map = solved[..., :HEAD]
-    local_pull = solved[..., HEAD:]
-    read_unit = pair_scores(forward, back_unit) * causal_incl * -learn_rate[:, :, None, :]
-    read_key = pair_scores(forward, back_key) * causal_incl
-    local_out = apply_scores(read_unit, local_pull) + apply_scores(read_key, values)
-    read_start = forward * joined + apply_scores(read_unit, carry_map)
-    block_total = cumulative[:, :, -1:, :]
-    tail_mask = (doc_blocks == doc_blocks[:, -1:]).astype(jnp.float32)[:, None, :, None]
-    end_unit = unit_keys * jnp.exp(block_total - cumulative) * tail_mask * -learn_rate[..., None]
-    end_key = key_heads * jnp.exp(block_total - cumulative) * tail_mask
-    block_map = jnp.eye(HEAD, dtype=jnp.float32) * (jnp.exp(block_total) * joined[:, :, -1:, :])
-    block_map = block_map + jnp.einsum("bhsn,bhsm->bhnm", carry_map, end_unit, precision=highest)
-    block_add = jnp.einsum("bhsv,bhsm->bhvm", local_pull, end_unit, precision=highest)
-    block_add = block_add + jnp.einsum("bhsv,bhsm->bhvm", values, end_key, precision=highest)
-    identity_map = jnp.broadcast_to(jnp.eye(HEAD, dtype=jnp.float32), (head_number, HEAD, HEAD))
-    carried = jnp.zeros((head_number, HEAD, HEAD), jnp.float32)
-    through = identity_map
-    outputs = []
-    starts = []
-    for block_index in range(block_list):
-        outputs.append(
-            local_out[block_index]
-            + jnp.einsum("hlm,hvm->hlv", read_start[block_index], carried, precision=highest)
-        )
-        starts.append(
-            jnp.einsum("hlm,hnm->hln", read_start[block_index], through, precision=highest)
-        )
-        carried = (
-            jnp.einsum("hvn,hnm->hvm", carried, block_map[block_index], precision=highest)
-            + block_add[block_index]
-        )
-        through = jnp.einsum("hvn,hnm->hvm", through, block_map[block_index], precision=highest)
-    first_doc = jnp.full((8, 2 * HEAD), documents[0].astype(jnp.float32))
-    last_doc = jnp.full((8, 2 * HEAD), documents[-1].astype(jnp.float32))
-    pairs = head_number // 2
-    zero_block = jnp.zeros((pairs, HEAD, HEAD), jnp.float32)
-    maps = through.reshape(pairs, 2, HEAD, HEAD)
-    maps = jnp.concatenate(
-        [
-            jnp.concatenate([maps[:, 0], zero_block], -1),
-            jnp.concatenate([zero_block, maps[:, 1]], -1),
-        ],
-        1,
-    )
-    adds = carried.reshape(pairs, 2, HEAD, HEAD)
-    arriving, prior = chain_states(
-        maps, jnp.concatenate([adds[:, 0], adds[:, 1]], -1), first_doc, last_doc
-    )
-    joined_here = (prior[0, 0] == first_doc[0, 0]).astype(jnp.float32)
-    incoming = jnp.stack([arriving[..., :HEAD], arriving[..., HEAD:]], 1).reshape(
-        head_number, HEAD, HEAD
-    )
-    incoming = incoming.astype(jnp.float32) * joined_here
-    head_read = jnp.stack(outputs) + jnp.einsum(
-        "bhln,hvn->bhlv", jnp.stack(starts), incoming, precision=highest
-    )
-    centre = jnp.mean(head_read, -1, keepdims=True)
-    spread = jnp.mean(jnp.square(head_read - centre), -1, keepdims=True)
-    normed = (
-        ((head_read - centre) * lax.rsqrt(spread + group_eps))
-        .transpose(0, 2, 1, 3)
-        .reshape(length, local_width)
-    )
-    return (normed * head_norm_scale).astype(jnp.bfloat16)
-
-
 def per_device(
     head_queries,
     head_keys,
@@ -560,7 +810,7 @@
     common_up_weight,
     common_down_weight,
 ):
-    head_outputs = linear_recurrence_mixer(
+    head_outputs = mixer(
         head_queries,
         head_keys,
         head_values,

time: 220 us -> 147 us (0.67); the launches traced: 216 us -> 146 us
  matrix products: 66.4 us -> 22.3 us
  local copies, waits for them, and re-layouts: 21.8 us -> 5.11 us
  other arithmetic: 14.6 us -> 4.57 us
  Pallas kernels: 111 us -> 114 us
  between operations: 2.91 us -> 0.24 us
    dot_general x39 -> x0, matrix products: 44.2 us -> none  [the longest x15 17.2 us: apply_scores(): return jnp.einsum('bhts,bhsn->bhtn', scores, operand, precision=highest)]
    pallas_call x1, Pallas kernels: 10.2 us -> 20.7 us  [mixer(): pl.pallas_call(lambda *refs: mixer_kernel(size, *refs), out_shape=jax.Sha...]
    reshape x9 -> x0, local copies, waits for them, and re-layouts: 8.22 us -> none  [the longest x3 6.49 us: split_heads(): return values.astype(jnp.float32).reshape(block_list, BLOCK_SPAN, head_nu...]
    pallas_call x1, Pallas kernels: 52.4 us -> 45 us  [dispatch(): pl.pallas_call(lambda *refs: dispatch_kernel(size, groups, *refs), out_sh...]
    transpose x3 -> x0, local copies, waits for them, and re-layouts: 4.64 us -> none  [the longest x2 3.34 us: split_heads(): return values.astype(jnp.float32).reshape(block_list, BLOCK_SPAN, head_nu...]
    slice x5 -> x0, local copies, waits for them, and re-layouts: 2.72 us -> none  [the longest x1 1.19 us: linear_recurrence_mixer(): joined_here = (prior[0, 0] == first_doc[0, 0]).astype(jnp.float32)]
    concatenate x3 -> x0, other arithmetic: 2.29 us -> none  [the longest x1 0.81 us: linear_recurrence_mixer(): jnp.concatenate([jnp.concatenate([maps[:, 0], zero_block], -1), jnp.conca...]
    unnamed x71 -> x23, local copies, waits for them, and re-layouts: 2.71 us -> 4.74 us
where the time goes in v1:
time: 147 us; the launch traced here: 146 us
  Pallas kernels  114 us (78%)
  matrix products  22.3 us (15%)
  local copies, waits for them, and re-layouts  5.11 us (3%)
  other arithmetic  4.57 us (3%)
    pallas_call x1, Pallas kernels, dispatch(): pl.pallas_call(lambda *refs: dispatch_kernel(size, groups, *refs), out_sh...  45 us
    pallas_call x1, Pallas kernels, tp_reduce_return(): pl.pallas_call(lambda parts_ref, extra_ref, *refs: tp_reduce_kernel(size,...  35.9 us
    pallas_call x1, Pallas kernels, mixer(): pl.pallas_call(lambda *refs: mixer_kernel(size, *refs), out_shape=jax.Sha...  20.7 us
    pallas_call x1, Pallas kernels, tp_reduce(): pl.pallas_call(lambda *refs: tp_reduce_kernel(size, 1, False, *refs), out...  12.1 us
    unnamed x23, local copies, waits for them, and re-layouts  4.74 us
    dot_general x2, matrix products, per_device(): jnp.dot(rows_in, routed_gate_weight[expert], preferred_element_type=jnp.f...  4.42 us
    dot_general x1, matrix products, per_device(): jnp.dot(jnp.concatenate(hidden_list, -1), routed_down_weight.reshape(-1,...  3.51 us
    dot_general x1, matrix products, per_device(): jnp.dot(head_outputs, mixer_output_weight, preferred_element_type=jnp.flo...  3.43 us

profile of v1, /device:TPU:0, one launch (start us, length us, event | category | flops | bytes accessed | tf_op | source)
XLA Modules:
  0.0 146.0 jit_solution(487352742022860033)
XLA Ops:
  0.0 1.0 copy.29
  1.0 0.1 reshape.75
  1.1 0.1 fusion.20
  1.3 0.3 reduce_window_sum.11
  1.5 0.2 select_reduce_fusion
  1.8 0.1 eq.49
  1.9 0.1 copy.30
  2.0 0.1 fusion.27
  2.1 1.5 %copy.28.refs_5_ = f32[256,8]{1,0:T(8,128)} copy(f32[256,8]{0,1:T(8,128)} %param.24) | data formatting | bytes 16384 | tf_op args[5]
  3.6 1.4 copy.27.refs_4_
  5.0 20.7 %shard_map.181 = bf16[256,512]{1,0:T(8,128)(2,1)} custom-call(bf16[256,512]{1,0:T(8,128)(2,1)} %refs_0_.1, bf16[256,512]{1,0:T(8,128)(2,1)} %refs_1_.1, bf16[256,512]{1,0:T(8,128)(2,1)} %refs_2_.1, bf16[256,512]{1,0:T(8,128)(2,1)} %refs_3_.1, bf16[256,8]{1,0:T(8,128)(2,1)} %copy.27.refs_4_, f32[256,8]{1,0:T(8,128)} %copy.28.refs_5_, s32[1,256]{1,0:T(1,128)} %bitcast.55, ...), custom_call_target="tpu_custom_call" | custom-call | tf_op jit(solution)/shard_map/pallas_call | solution.py:493
  25.8 0.0 copy-start.4
  25.8 3.4 %convolution_convert_fusion.2 = bf16[256,2048]{1,0:T(8,128)(2,1)} fusion(bf16[256,512]{1,0:T(8,128)(2,1)} %shard_map.181, bf16[512,2048]{1,0:T(8,128)(2,1)} %param.28), kind=kOutput, calls=%fused_computation.2 | convolution fusion | flops 537395200 | bytes 3407872 | tf_op jit(solution)/shard_map/dot_general | solution.py:827
  29.2 12.1 %shard_map.182 = f32[4,16,2048]{2,1,0:T(8,128)} custom-call(bf16[4,4,16,2048]{3,2,1,0:T(8,128)(2,1)} %bitcast.50), custom_call_target="tpu_custom_call" | custom-call | tf_op jit(solution)/shard_map/pallas_call | solution.py:644
  41.4 1.2 fusion.21
  42.6 1.3 multiply_reduce_fusion
  43.9 1.2 multiply_convert_fusion.refs_1_
  45.1 0.0 copy-start.2
  45.1 1.3 convolution_convert_fusion.3
  46.4 45.0 %shard_map.183 = (bf16[4,8,24,2048]{3,2,1,0:T(8,128)(2,1)}, bf16[4,64,2048]{2,1,0:T(8,128)(2,1)}) custom-call(bf16[8,24,2048]{2,1,0:T(8,128)(2,1)} %bitcast.52, bf16[64,2048]{1,0:T(8,128)(2,1)} %copy-done.2), custom_call_target="tpu_custom_call" | custom-call | tf_op jit(solution)/shard_map/pallas_call | solution.py:777
  91.4 1.9 %fusion.35 = f32[256,128]{1,0:T(8,128)S(1)} fusion(bf16[256,2048]{1,0:T(8,128)(2,1)} %bitcast.47, bf16[2048,128]{1,0:T(8,128)(2,1)} %param.35), kind=kOutput, calls=%fused_computation.61 | convolution fusion | flops 134217728 | bytes 1703936 | tf_op jit(solution)/shard_map/dot_general | solution.py:871
  93.3 3.0 %convolution_convert_fusion.1 = bf16[256,2048]{1,0:T(8,128)(2,1)} fusion(bf16[128,2048]{1,0:T(8,128)(2,1)} %param.37, bf16[256,2048]{1,0:T(8,128)(2,1)S(1)} %bitcast.48, bf16[2048,128]{1,0:T(8,128)(2,1)} %param.36, f32[256,128]{1,0:T(8,128)S(1)} %fusion.35), kind=kOutput, calls=%fused_computation.1 | convolution fusion | flops 269156352 | bytes 3276800 | tf_op jit(solution)/shard_map/dot_general | solution.py:874
  96.2 3.3 %fusion.11 = f32[768,256]{0,1:T(8,128)S(1)} fusion(bf16[768,2048]{1,0:T(8,128)(2,1)} %bitcast.56, bf16[2,2048,256]{2,1,0:T(8,128)(2,1)} %param.32), kind=kOutput, calls=%fused_computation.19 | convolution fusion | flops 805306368 | bytes 4980736 | tf_op jit(solution)/shard_map/dot_general | solution.py:859
  99.6 0.4 copy-done.9
  100.0 1.2 fusion.5
  101.2 0.4 copy-done.8
  101.6 1.1 fusion.8
  102.7 1.2 fusion.4
  103.9 3.5 %convolution_convert_fusion = bf16[768,2048]{1,0:T(8,128)(2,1)} fusion(bf16[512,2048]{1,0:T(8,128)(2,1)S(1)} %bitcast.46, bf16[768,256]{0,1:T(8,128)(2,1)S(1)} %fusion.4, bf16[768,256]{0,1:T(8,128)(2,1)S(1)} %fusion.5), kind=kOutput, calls=%fused_computation | convolution fusion | flops 1613758464 | bytes 6029312 | tf_op jit(solution)/shard_map/dot_general | solution.py:865
  107.4 35.9 %shard_map.184 = (bf16[8,24,2048]{2,1,0:T(8,128)(2,1)}, f32[64,2048]{1,0:T(8,128)}) custom-call(bf16[4,8,24,2048]{3,2,1,0:T(8,128)(2,1)} %bitcast.51, bf16[4,1,64,2048]{3,2,1,0:T(8,128)(2,1)} %bitcast.49), custom_call_target="tpu_custom_call" | custom-call | tf_op jit(solution)/shard_map/pallas_call | solution.py:664
  143.3 0.1 select_reduce_fusion.1
  143.4 2.5 %fusion.1 = bf16[64,2048]{1,0:T(8,128)(2,1)} fusion(f32[64,2048]{1,0:T(8,128)} %get-tuple-element.12, f32[64,192]{1,0:T(8,128)S(1)} %select_reduce_fusion.1, bf16[192,2048]{1,0:T(8,128)(2,1)} %bitcast.53, bf16[64,2048]{1,0:T(8,128)(2,1)S(1)} %copy-done.3), kind=kOutput, calls=%fused_computation.6 | convolution fusion | flops 302645248 | bytes 1884160 | tf_op jit(solution)/shard_map/dot_general | solution.py:882
  (22 shorter events, 0.1 us)
Async XLA Ops:
  0.0 103.9 %copy-start = (bf16[2,256,2048]{2,1,0:T(8,128)(2,1)S(1)}, bf16[2,256,2048]{2,1,0:T(8,128)(2,1)}, u32[]{:S(2)}) copy-start(bf16[2,256,2048]{2,1,0:T(8,128)(2,1)} %param.34) | copy-start | bytes 6291460
  25.8 15.6 %copy-start.4 = (bf16[64,2048]{1,0:T(8,128)(2,1)S(1)}, bf16[64,2048]{1,0:T(8,128)(2,1)}, u32[]{:S(2)}) copy-start(bf16[64,2048]{1,0:T(8,128)(2,1)} %param.26) | copy-start | bytes 786436
  29.2 14.7 %copy-start.5 = (f32[2048]{0:T(1024)S(1)}, f32[2048]{0:T(1024)}, u32[]{:S(2)}) copy-start(f32[2048]{0:T(1024)} %param.29) | copy-start | bytes 24580
  45.1 1.3 copy-start.2
  91.4 1.9 %copy-start.1 = (bf16[4,64,2048]{2,1,0:T(8,128)(2,1)S(1)}, bf16[4,64,2048]{2,1,0:T(8,128)(2,1)}, u32[]{:S(2)}) copy-start(bf16[4,64,2048]{2,1,0:T(8,128)(2,1)} %get-tuple-element.10) | copy-start | bytes 3145732
  96.2 3.4 %copy-start.7 = (bf16[4,8,24,2048]{3,2,1,0:T(8,128)(2,1)S(1)}, bf16[4,8,24,2048]{3,2,1,0:T(8,128)(2,1)}, u32[]{:S(2)}) copy-start(bf16[4,8,24,2048]{3,2,1,0:T(8,128)(2,1)} %get-tuple-element.9) | copy-start | bytes 9437188
  96.2 3.8 %copy-start.9 = (bf16[2,2048,256]{2,1,0:T(8,128)(2,1)S(1)}, bf16[2,2048,256]{2,1,0:T(8,128)(2,1)}, u32[]{:S(2)}) copy-start(bf16[2,2048,256]{2,1,0:T(8,128)(2,1)} %param.33) | copy-start | bytes 6291460
  100.0 1.6 %copy-start.8 = (bf16[2,2048,256]{2,1,0:T(8,128)(2,1)S(1)}, bf16[2,2048,256]{2,1,0:T(8,128)(2,1)}, u32[]{:S(2)}) copy-start(bf16[2,2048,256]{2,1,0:T(8,128)(2,1)} %param.32) | copy-start | bytes 6291460
  107.4 35.9 %copy-start.6 = (f32[64,2]{0,1:T(2,128)S(1)}, f32[64,2]{0,1:T(2,128)}, u32[]{:S(2)}) copy-start(f32[64,2]{0,1:T(2,128)} %param.31) | copy-start | bytes 1540
  107.4 36.0 %copy-start.3 = (bf16[64,2048]{1,0:T(8,128)(2,1)S(1)}, bf16[64,2048]{1,0:T(8,128)(2,1)}, u32[]{:S(2)}) copy-start(bf16[64,2048]{1,0:T(8,128)(2,1)} %copy-done.2) | copy-start | bytes 786436

commit v2 on v1

--- a/solution.py
+++ b/solution.py
@@ -16,6 +16,8 @@
 group_eps = 0.00064
 norm_eps = 1e-05
 unit_eps = 1e-06
+CLOSE = 2
+EXTRA_TURN = 5
 SCORE_PRECISION = lax.Precision.HIGH
 
 
@@ -656,137 +658,442 @@
     )(parts)
 
 
-def tp_reduce_return(parts, extra):
-    size, pieces, rows, width = parts.shape
-    more = extra.shape[1]
-    half = size // 2
-    kind = jnp.bfloat16
-    return pl.pallas_call(
-        lambda parts_ref, extra_ref, *refs: tp_reduce_kernel(
-            size, pieces, True, parts_ref, extra_ref, *refs
-        ),
-        out_shape=(
-            jax.ShapeDtypeStruct((pieces, rows, width), kind),
-            jax.ShapeDtypeStruct((more, width), jnp.float32),
-        ),
-        in_specs=[VMEM, VMEM],
-        out_specs=(VMEM, VMEM),
-        scratch_shapes=[
-            pltpu.VMEM((half, pieces, rows, width), kind),
-            pltpu.VMEM((half - 1, pieces, rows, width), kind),
-            pltpu.VMEM((half - 1, pieces, rows, width), kind),
-            pltpu.VMEM((half, 1, more, width), kind),
-            pltpu.VMEM((half - 1, 1, more, width), kind),
-            pltpu.VMEM((half - 1, 1, more, width), kind),
-            pltpu.VMEM((pieces, rows, width), kind),
-        ]
-        + [pltpu.SemaphoreType.DMA((pieces + 1, half))] * 4
-        + [pltpu.SemaphoreType.DMA((pieces,))] * 2,
-        compiler_params=pltpu.CompilerParams(
-            collective_id=3, has_side_effects=True, vmem_limit_bytes=60 * 1024 * 1024
-        ),
-    )(parts, extra[:, None])
-
-
-def dispatch_kernel(
-    size, groups, outgoing, stream, arrived, rows_all, local, asend, arecv, nsend, nrecv, fsend, frecv, gsend, grecv
+def flip(index, bits, size):
+    total = 0
+    place = 1
+    while place < size:
+        total = total + lax.rem(lax.div(index, place) + lax.div(bits, place), 2) * place
+        place = place * 2
+    return total
+
+
+def moe_kernel(
+    size,
+    groups,
+    capacity,
+    block,
+    choice,
+    stream,
+    mix,
+    gate,
+    upward,
+    down,
+    common_gate,
+    common_up,
+    common_down,
+    out,
+    outgoing,
+    near_out,
+    mix_far,
+    returned_far,
+    stage_far,
+    arrived,
+    rows_all,
+    parts,
+    near,
+    pair,
+    far,
+    stage,
+    returned,
+    extra,
+    enear,
+    epair,
+    efar,
+    gate_v,
+    up_v,
+    down_v,
+    cgate_v,
+    cup_v,
+    cdown_v,
+    local,
+    loads,
+    asend,
+    arecv,
+    nsend,
+    nrecv,
+    fsend,
+    frecv,
+    gsend,
+    grecv,
+    rnsend,
+    rnrecv,
+    rfsend,
+    rfrecv,
+    bsend,
+    brecv,
+    msend,
+    mrecv,
 ):
     me = lax.axis_index("tp")
     own = lax.axis_index("sp")
     half = size // 2
     partner = me + 1 - 2 * lax.rem(me, 2)
+    tokens, width = stream.shape
+    close = min(CLOSE, groups)
+    batch = max(1, groups // 8)
+    steps = groups // batch
+    fetches = [
+        pltpu.make_async_copy(src, dst, loads.at[i])
+        for i, (src, dst) in enumerate(
+            (
+                (common_gate, cgate_v),
+                (common_up, cup_v),
+                (common_down, cdown_v),
+                (gate, gate_v),
+                (upward, up_v),
+                (down, down_v),
+            )
+        )
+    ]
+    for fetch in fetches:
+        fetch.start()
+    keep_rows = pltpu.make_async_copy(stream, rows_all.at[me], local.at[1])
+    keep_rows.start()
+    returned_far[...] = jnp.zeros_like(returned_far)
+    outgoing[...] = narrow(mm(narrow(choice[me]), stream[...])).reshape(groups, block, width)
     greet((("tp", size), ("sp", groups)))
 
-    def exchange(step):
+    def ahead(j):
+        return lax.rem(me + 2 * j, size)
+
+    def exchange(k, j=0, near=False):
+        other = flip(own, k, groups)
         return remote(
-            outgoing.at[lax.rem(own + step, groups)],
-            arrived.at[me, own],
-            asend.at[step],
-            arecv.at[step],
+            near_out.at[k, j] if near else outgoing.at[other],
+            arrived.at[ahead(j), k],
+            asend.at[k, j],
+            arecv.at[k, j],
             "sp",
-            lax.rem(own + step, groups),
+            other,
         )
 
-    def place(step, who):
-        if step == groups:
-            return rows_all.at[who]
-        return arrived.at[who, lax.rem(own - step + groups, groups)]
-
-    def source(step):
-        if step == groups:
-            return stream
-        return outgoing.at[own] if step == 0 else place(step, me)
-
-    def near_copy(step):
-        return remote(source(step), place(step, me), nsend.at[step], nrecv.at[step], "tp", partner)
-
-    def far_copy(step, k):
+    def send_mix(j):
+        return remote(mix, mix_far.at[j - 1], msend.at[j], mrecv.at[j], "tp", ahead(size - j))
+
+    def place(k, who, whole):
+        return rows_all.at[who] if whole else arrived.at[who, k]
+
+    def near_copy(k, whole=False):
+        src = stream if whole else arrived.at[me, k]
+        return remote(src, place(k, me, whole), nsend.at[k], nrecv.at[k], "tp", partner)
+
+    def far_copy(k, j, whole=False):
+        src = stream if whole else arrived.at[me, k]
         return remote(
-            source(step),
-            place(step, me),
-            fsend.at[step, k],
-            frecv.at[step, k],
+            src, place(k, me, whole), fsend.at[k, j], frecv.at[k, j], "tp", lax.rem(me + 2 * j, size)
+        )
+
+    def forward(k, j, whole=False):
+        ref = place(k, lax.rem(me - 2 * j + size, size), whole)
+        return remote(ref, ref, gsend.at[k, j], grecv.at[k, j], "tp", partner)
+
+    def send_own(k, whole=False):
+        for j in range(1, half):
+            far_copy(k, j, whole).start()
+        near_copy(k, whole).start()
+
+    def pass_on(k, whole=False):
+        for j in range(1, half):
+            far_copy(k, j, whole).wait_recv()
+            forward(k, j, whole).start()
+
+    def gathered(k, whole=False):
+        near_copy(k, whole).wait_recv()
+        for j in range(1, half):
+            forward(k, j, whole).wait_recv()
+
+    def reduce_near(k, j, whole=False):
+        src, dst = (extra, enear) if whole else (parts, near)
+        index = 0 if whole else k
+        return remote(
+            src.at[lax.rem(partner + 2 * j, size), index],
+            dst.at[j, index],
+            rnsend.at[k, j],
+            rnrecv.at[k, j],
             "tp",
-            lax.rem(me + 2 * k, size),
+            partner,
         )
 
-    def forward(step, k):
-        who = place(step, lax.rem(me - 2 * k + size, size))
-        return remote(who, who, gsend.at[step, k], grecv.at[step, k], "tp", partner)
-
-    def start_own(step):
-        for k in range(1, half):
-            far_copy(step, k).start()
-        near_copy(step).start()
-
-    def pass_on(step):
-        for k in range(1, half):
-            far_copy(step, k).wait_recv()
-            forward(step, k).start()
-
-    keep_block = pltpu.make_async_copy(outgoing.at[own], arrived.at[me, own], local.at[0])
-    keep_rows = pltpu.make_async_copy(stream, rows_all.at[me], local.at[1])
-    for step in range(1, groups):
-        exchange(step).start()
-    keep_block.start()
-    keep_rows.start()
-    order = [groups] + list(range(groups))
-    for turn, step in enumerate(order):
-        if 0 < step < groups:
-            exchange(step).wait_recv()
-        start_own(step)
-        if turn > 0:
-            pass_on(order[turn - 1])
-    pass_on(order[-1])
-    keep_block.wait()
+    def reduce_far(k, j, whole=False):
+        src, dst = (epair, efar) if whole else (pair, far)
+        index = 0 if whole else k
+        return remote(
+            src.at[j - 1, index],
+            dst.at[j - 1, index],
+            rfsend.at[k, j],
+            rfrecv.at[k, j],
+            "tp",
+            lax.rem(me + 2 * j, size),
+        )
+
+    def back(k, j=0, whose=None):
+        other = flip(own, k, groups)
+        where = own if whose is None else whose
+        return remote(
+            stage.at[k] if j == 0 else stage_far.at[j - 1, k],
+            returned.at[where] if j == 0 else returned_far.at[j - 1, where],
+            bsend.at[k, j],
+            brecv.at[k, j],
+            "sp",
+            other,
+        )
+
+    def finish_close(k):
+        for j in range(half):
+            reduce_near(k, j).wait_recv()
+            total = narrow(
+                parts[ahead(j), k].astype(jnp.float32) + near[j, k].astype(jnp.float32)
+            )
+
+            @pl.when(k == 0)
+            def _():
+                if j == 0:
+                    returned[own] = total
+                else:
+                    returned_far[j - 1, own] = total
+
+            @pl.when(k > 0)
+            def _():
+                if j == 0:
+                    stage[k] = total
+                else:
+                    stage_far[j - 1, k] = total
+                back(k, j).start()
+
+    def weighed(weights, rows):
+        top, rest = split(weights)
+        rows = narrow(rows.astype(jnp.float32).reshape(groups * block, width))
+        return mm(top, rows) + mm(rest, rows)
+
+    def add_extra():
+        for k in range(1, close):
+            for j in range(half):
+                back(k, j, flip(own, k, groups)).wait_recv()
+        for j in range(1, half):
+            reduce_near(groups, j, True).wait_recv()
+            send_mix(j).wait_recv()
+            epair[j - 1, 0] = narrow(
+                extra[ahead(j), 0].astype(jnp.float32)
+                + enear[j, 0].astype(jnp.float32)
+                + weighed(mix_far[j - 1], returned_far[j - 1])
+            )
+            reduce_far(groups, j, True).start()
+
+    def start_reduce(k, whole=False):
+        for j in range(half - 1, -1, -1):
+            reduce_near(k, j, whole).start()
+
+    def add_pair(k, whole=False):
+        src, got, to = (extra, enear, epair) if whole else (parts, near, pair)
+        index = 0 if whole else k
+        for j in range(1, half):
+            reduce_near(k, j, whole).wait_recv()
+            to[j - 1, index] = narrow(
+                src[lax.rem(me + 2 * j, size), index].astype(jnp.float32)
+                + got[j, index].astype(jnp.float32)
+            )
+            reduce_far(k, j, whole).start()
+
+    def total_of(k, whole=False):
+        src, got, last = (extra, enear, efar) if whole else (parts, near, far)
+        index = 0 if whole else k
+        reduce_near(k, 0, whole).wait_recv()
+        total = src[me, index].astype(jnp.float32) + got[0, index].astype(jnp.float32)
+        for j in range(1, half):
+            reduce_far(k, j, whole).wait_recv()
+            total = total + last[j - 1, index].astype(jnp.float32)
+        return total
+
+    def swish(gated, lifted):
+        return gated / (1.0 + jnp.exp(-gated)) * lifted
+
+    lead, relay = min(4, steps), min(2, steps)
+    send_own(groups, True)
+    for k in range(close, groups):
+        exchange(k).start()
+    for j in range(1, half):
+        send_mix(j).start()
     keep_rows.wait()
-    for step in range(1, groups):
-        exchange(step).wait_send()
-    for step in order:
-        near_copy(step).wait()
-        for k in range(1, half):
-            far_copy(step, k).wait_send()
-            forward(step, k).wait()
-
-
-def dispatch(outgoing, stream):
+    pass_on(groups, True)
+    for k in range(1, close):
+        other = flip(own, k, groups)
+        for j in range(half):
+            picked = narrow(choice[ahead(j), pl.ds(pl.multiple_of(other * block, 8), block)])
+            near_out[k, j] = narrow(mm(picked, rows_all[ahead(j)]))
+            exchange(k, j, True).start()
+    for k in range(close, lead * batch):
+        exchange(k).wait_recv()
+        send_own(k)
+    gathered(groups, True)
+    for who in range(size):
+        picked = narrow(choice[who, pl.ds(pl.multiple_of(own * block, 8), block)])
+        arrived[who, 0] = narrow(mm(picked, rows_all[who]))
+    for fetch in fetches[:3]:
+        fetch.wait()
+    everyone = rows_all[...].reshape(size * tokens, width)
+    hidden = narrow(swish(mm(everyone, cgate_v[...]), mm(everyone, cup_v[...])))
+    extra[...] = narrow(mm(hidden, cdown_v[...])).reshape(size, 1, tokens, width)
+    start_reduce(groups, True)
+    for k in range(1, close):
+        for j in range(half):
+            exchange(k, j, True).wait_recv()
+        near_copy(k).start()
+        for j in range(1, half):
+            forward(k, j).start()
+    for k in range(close, relay * batch):
+        pass_on(k)
+    for fetch in fetches[3:]:
+        fetch.wait()
+
+    piece_rows = size * batch * block
+    row = lax.broadcasted_iota(jnp.int32, (piece_rows, gate_v.shape[2]), 0)
+    hosted = lax.div(lax.rem(row, block), capacity)
+
+    def turn(t, carry):
+        def each(base, action):
+            for b in range(batch):
+                action(base * batch + b)
+
+        @pl.when(t + lead < steps)
+        def _():
+            def action(k):
+                exchange(k).wait_recv()
+                send_own(k)
+
+            each(t + lead, action)
+
+        @pl.when(t + relay < steps)
+        def _():
+            each(t + relay, pass_on)
+
+        @pl.when(t < steps)
+        def _():
+            def arrive(k):
+                @pl.when(k > 0)
+                def _():
+                    gathered(k)
+
+            each(t, arrive)
+            rows_in = narrow(
+                arrived[:, pl.ds(t * batch, batch)].astype(jnp.float32).reshape(piece_rows, width)
+            )
+            hidden = []
+            for expert in range(EXP_DEV):
+                gated = mm(rows_in, gate_v[expert])
+                lifted = mm(rows_in, up_v[expert])
+                hidden.append(narrow(jnp.where(hosted == expert, swish(gated, lifted), 0.0)))
+            part = mm(jnp.concatenate(hidden, 1), down_v[...].reshape(-1, width))
+            parts[:, pl.ds(t * batch, batch)] = narrow(
+                part.reshape(size, batch, block, width)
+            )
+            each(t, start_reduce)
+
+        @pl.when((t >= 1) & (t <= steps))
+        def _():
+            def action(k):
+                @pl.when(k < close)
+                def _():
+                    finish_close(k)
+
+                @pl.when(k >= close)
+                def _():
+                    add_pair(k)
+
+            each(t - 1, action)
+
+        @pl.when(t == min(EXTRA_TURN, steps + 1))
+        def _():
+            add_extra()
+
+        @pl.when(t >= 2)
+        def _():
+            def action(k):
+                @pl.when(k >= close)
+                def _():
+                    stage[k] = narrow(total_of(k))
+                    back(k).start()
+
+            each(t - 2, action)
+
+        return carry
+
+    lax.fori_loop(0, steps + 2, turn, 0)
+
+    shared = total_of(groups, True)
+    for k in range(close, groups):
+        back(k, 0, flip(own, k, groups)).wait_recv()
+    out[...] = narrow(
+        residual_scale * stream[...].astype(jnp.float32)
+        + weighed(mix[...], returned[...])
+        + shared
+    )
+
+    for k in range(1, groups):
+        for j in range(half if k < close else 1):
+            exchange(k, j, k < close).wait_send()
+            back(k, j).wait_send()
+    for k in range(groups + 1):
+        whole = k == groups
+        for j in range(half):
+            reduce_near(k, j, whole).wait_send()
+        if k > 0:
+            near_copy(k, whole).wait_send()
+        for j in range(1, half):
+            if k > 0:
+                forward(k, j, whole).wait_send()
+            if k >= close:
+                far_copy(k, j, whole).wait_send()
+                reduce_far(k, j, whole).wait_send()
+    for j in range(1, half):
+        send_mix(j).wait_send()
+
+
+def moe(
+    choice, stream, mix, gate, upward, down, common_gate, common_up, common_down, capacity, block
+):
     size = lax.axis_size("tp")
-    groups, rows, width = outgoing.shape
+    groups = lax.axis_size("sp")
+    tokens, width = stream.shape
+    close = min(CLOSE, groups)
     half = size // 2
     dma = pltpu.SemaphoreType.DMA
+    b16, f32 = jnp.bfloat16, jnp.float32
+    anywhere = pl.BlockSpec(memory_space=pl.ANY)
+    weights = (gate, upward, down, common_gate, common_up, common_down)
     return pl.pallas_call(
-        lambda *refs: dispatch_kernel(size, groups, *refs),
-        out_shape=(
-            jax.ShapeDtypeStruct((size, groups, rows, width), jnp.bfloat16),
-            jax.ShapeDtypeStruct((size,) + stream.shape, jnp.bfloat16),
+        lambda *refs: moe_kernel(size, groups, capacity, block, *refs),
+        out_shape=jax.ShapeDtypeStruct((tokens, width), b16),
+        in_specs=[VMEM] * 3 + [anywhere] * 6,
+        out_specs=VMEM,
+        scratch_shapes=[
+            pltpu.VMEM((groups, block, width), b16),
+            pltpu.VMEM((close, half, block, width), b16),
+            pltpu.VMEM((half - 1,) + mix.shape, f32),
+            pltpu.VMEM((half - 1, groups, block, width), b16),
+            pltpu.VMEM((half - 1, close, block, width), b16),
+            pltpu.VMEM((size, groups, block, width), b16),
+            pltpu.VMEM((size, tokens, width), b16),
+            pltpu.VMEM((size, groups, block, width), b16),
+            pltpu.VMEM((half, groups, block, width), b16),
+            pltpu.VMEM((half - 1, groups, block, width), b16),
+            pltpu.VMEM((half - 1, groups, block, width), b16),
+            pltpu.VMEM((groups, block, width), b16),
+            pltpu.VMEM((groups, block, width), b16),
+            pltpu.VMEM((size, 1, tokens, width), b16),
+            pltpu.VMEM((half, 1, tokens, width), b16),
+            pltpu.VMEM((half - 1, 1, tokens, width), b16),
+            pltpu.VMEM((half - 1, 1, tokens, width), b16),
+        ]
+        + [pltpu.VMEM(w.shape, b16) for w in weights]
+        + [dma((2,)), dma((6,)), dma((groups, half)), dma((groups, half))]
+        + [dma((groups + 1,))] * 2
+        + [dma((groups + 1, half))] * 8
+        + [dma((groups, half))] * 2
+        + [dma((half,))] * 2,
+        compiler_params=pltpu.CompilerParams(
+            collective_id=4, has_side_effects=True, vmem_limit_bytes=60 * 1024 * 1024
         ),
-        in_specs=[VMEM, VMEM],
-        out_specs=(VMEM, VMEM),
-        scratch_shapes=[dma((2,)), dma((groups,)), dma((groups,))]
-        + [dma((groups + 1,))] * 2
-        + [dma((groups + 1, half))] * 4,
-        compiler_params=pltpu.CompilerParams(collective_id=4, has_side_effects=True),
-    )(outgoing, stream)
+    )(choice, stream, mix, *weights)
 
 
 def per_device(
@@ -838,53 +1145,34 @@
     )
     experts = EXP_DEV * groups
     capacity = max(2, (3 * TOK_DEV * TOP + 2 * experts - 1) // (2 * experts))
+    block_rows = 8 * ((EXP_DEV * capacity + 7) // 8)
     chosen = routes.reshape(quarters, own_rows * TOP)
     onehot = (chosen[..., None] == jnp.arange(experts, dtype=jnp.int32)).astype(jnp.int32)
     ranking = jnp.sum(jnp.cumsum(onehot, 1) * onehot, -1) - 1
-    slot_index = chosen * capacity + ranking
+    slot_index = (
+        chosen // EXP_DEV * block_rows + chosen % EXP_DEV * capacity + ranking
+    )
+    slot_index = slot_index.reshape(quarters, own_rows, TOP)
     own_slots = lax.dynamic_index_in_dim(slot_index, lax.axis_index("tp"), 0, keepdims=False)
-    own_slots = own_slots.reshape(own_rows, TOP)
-    slots = jnp.arange(experts * capacity, dtype=jnp.int32)
+    slots = jnp.arange(groups * block_rows, dtype=jnp.int32)
     hits = own_slots[:, :, None] == slots
-    spread_to = jnp.any(hits, 1).astype(jnp.bfloat16)
-    block_rows = EXP_DEV * capacity
-    outgoing = jnp.einsum(
-        "ts,td->sd", spread_to, stream, preferred_element_type=jnp.float32
-    ).astype(jnp.bfloat16)
-    arrived_all, rows_all = dispatch(outgoing.reshape(groups, block_rows, model_width), stream)
-    rows_in = arrived_all.reshape(quarters * groups * block_rows, model_width)
-    hosted = (jnp.arange(rows_in.shape[0], dtype=jnp.int32) % block_rows) // capacity
-    hidden_list = []
-    for expert in range(EXP_DEV):
-        gated = jnp.dot(rows_in, routed_gate_weight[expert], preferred_element_type=jnp.float32)
-        lifted = jnp.dot(rows_in, routed_up_weight[expert], preferred_element_type=jnp.float32)
-        hidden = (jax.nn.silu(gated) * lifted).astype(jnp.bfloat16)
-        hidden_list.append(
-            jnp.where((hosted == expert)[:, None], hidden, jnp.zeros_like(hidden))
-        )
-    partial_value = jnp.dot(
-        jnp.concatenate(hidden_list, -1),
-        routed_down_weight.reshape(-1, model_width),
-        preferred_element_type=jnp.float32,
-    ).astype(jnp.bfloat16)
-    rows_all = rows_all.reshape(quarters * own_rows, model_width)
-    shared_gated = jnp.dot(rows_all, common_gate_weight, preferred_element_type=jnp.float32)
-    shared_lifted = jnp.dot(rows_all, common_up_weight, preferred_element_type=jnp.float32)
-    shared_hidden = (jax.nn.silu(shared_gated) * shared_lifted).astype(jnp.bfloat16)
-    shared_part = jnp.dot(
-        shared_hidden, common_down_weight, preferred_element_type=jnp.float32
-    ).astype(jnp.bfloat16)
-    returned, shared_sum = tp_reduce_return(
-        partial_value.reshape(quarters, groups, block_rows, model_width),
-        shared_part.reshape(quarters, own_rows, model_width),
-    )
+    choice = jnp.zeros((quarters, groups * block_rows, own_rows), jnp.float32)
+    for route in range(TOP):
+        choice = choice + (slots[None, :, None] == slot_index[:, None, :, route])
     weights = jnp.sum(jnp.where(hits, routing_weight[:, :, None], 0.0), 1)
-    routed = jnp.dot(
+    return moe(
+        choice,
+        stream,
         weights,
-        returned.reshape(experts * capacity, model_width).astype(jnp.float32),
-        precision=lax.Precision.HIGHEST,
-    )
-    return (residual_scale * stream.astype(jnp.float32) + routed + shared_sum).astype(jnp.bfloat16)
+        routed_gate_weight,
+        routed_up_weight,
+        routed_down_weight,
+        common_gate_weight,
+        common_up_weight,
+        common_down_weight,
+        capacity,
+        block_rows,
+    )
 
 
 def solution(mesh):

time: 147 us -> 117 us (0.80)
  matrix products: 22.3 us -> 2.7 us
  Pallas kernels: 114 us -> 102 us
  other arithmetic: 4.57 us -> 6.58 us
    dot_general x9 -> x0, matrix products: 18.9 us -> none  [the longest x2 4.42 us: per_device(): jnp.dot(rows_in, routed_gate_weight[expert], preferred_element_type=jnp.f...]
    pallas_call x2 -> x1, Pallas kernels: 80.9 us -> 68.9 us  [moe(): pl.pallas_call(lambda *refs: moe_kernel(size, groups, capacity, block, *r...]
    unnamed x23 -> x14, local copies, waits for them, and re-layouts: 4.74 us -> 4.87 us
where the time goes in v2:
time: 117 us
  Pallas kernels  102 us (87%)
  other arithmetic  6.58 us (6%)
  local copies, waits for them, and re-layouts  5.31 us (5%)
  matrix products  2.7 us (2%)
    pallas_call x1, Pallas kernels, moe(): pl.pallas_call(lambda *refs: moe_kernel(size, groups, capacity, block, *r...  68.9 us
    pallas_call x1, Pallas kernels, mixer(): pl.pallas_call(lambda *refs: mixer_kernel(size, *refs), out_shape=jax.Sha...  20.7 us
    pallas_call x1, Pallas kernels, tp_reduce(): pl.pallas_call(lambda *refs: tp_reduce_kernel(size, 1, False, *refs), out...  12.1 us
    unnamed x14, local copies, waits for them, and re-layouts  4.87 us
    dot_general x1, matrix products, per_device(): jnp.dot(head_outputs, mixer_output_weight, preferred_element_type=jnp.flo...  2.7 us

profile of v2, /device:TPU:0, one launch (start us, length us, event | category | flops | bytes accessed | tf_op | source)
XLA Modules:
  0.0 116.5 jit_solution(8258616181027929757)
XLA Ops:
  0.0 0.0 copy-start
  0.0 1.6 %copy.53.refs_5_ = f32[256,8]{1,0:T(8,128)} copy(f32[256,8]{0,1:T(8,128)} %param.24) | data formatting | bytes 16384 | tf_op args[5]
  1.6 1.4 %copy.52.refs_4_ = bf16[256,8]{1,0:T(8,128)(2,1)} copy(bf16[256,8]{0,1:T(8,128)(2,1)} %param.23) | data formatting | bytes 8192 | tf_op args[4]
  3.0 20.7 %shard_map.181 = bf16[256,512]{1,0:T(8,128)(2,1)} custom-call(bf16[256,512]{1,0:T(8,128)(2,1)} %refs_0_.1, bf16[256,512]{1,0:T(8,128)(2,1)} %refs_1_.1, bf16[256,512]{1,0:T(8,128)(2,1)} %refs_2_.1, bf16[256,512]{1,0:T(8,128)(2,1)} %refs_3_.2, bf16[256,8]{1,0:T(8,128)(2,1)} %copy.52.refs_4_, f32[256,8]{1,0:T(8,128)} %copy.53.refs_5_, s32[1,256]{1,0:T(1,128)} %bitcast.25, ...), custom_call_target="tpu_custom_call" | custom-call | tf_op jit(solution)/shard_map/pallas_call | solution.py:495
  23.8 0.0 copy-done
  23.8 0.0 copy-start.1
  23.8 2.7 %convolution_convert_fusion = bf16[256,2048]{1,0:T(8,128)(2,1)} fusion(bf16[256,512]{1,0:T(8,128)(2,1)} %shard_map.181, bf16[512,2048]{1,0:T(8,128)(2,1)S(1)} %copy-done), kind=kOutput, calls=%fused_computation | convolution fusion | flops 537395200 | bytes 3407872 | tf_op jit(solution)/shard_map/dot_general | solution.py:1134
  26.5 0.0 copy-start.2
  26.5 0.0 copy-start.3
  26.5 12.1 %shard_map.182 = f32[4,16,2048]{2,1,0:T(8,128)} custom-call(bf16[4,4,16,2048]{3,2,1,0:T(8,128)(2,1)} %bitcast.21), custom_call_target="tpu_custom_call" | custom-call | tf_op jit(solution)/shard_map/pallas_call | solution.py:646
  38.7 0.0 copy-done.1
  38.7 0.0 copy-start.4
  38.7 1.2 %fusion.1 = f32[64]{0:T(128)S(1)} fusion(f32[4,16,2048]{2,1,0:T(8,128)} %shard_map.182, bf16[64,2048]{1,0:T(8,128)(2,1)S(1)} %copy-done.1), kind=kLoop, calls=%fused_computation.10 | loop fusion | flops 524224 | bytes 786688 | tf_op jit(solution)/shard_map/reduce_sum | solution.py:1141
  39.9 1.3 %multiply_reduce_fusion = f32[64]{0:T(128)S(1)} fusion(f32[64]{0:T(128)S(1)} %broadcast_multiply_fusion, f32[4,16,2048]{2,1,0:T(8,128)} %shard_map.182, bf16[64,2048]{1,0:T(8,128)(2,1)S(1)} %copy-done.1), kind=kLoop, calls=%fused_computation.3 | loop fusion | flops 786368 | bytes 786944 | tf_op jit(solution)/shard_map/reduce_sum | solution.py:1142
  41.2 0.0 copy-done.2
  41.2 1.9 %multiply_convert_fusion.refs_1_ = bf16[64,2048]{1,0:T(8,128)(2,1)} fusion(f32[2048]{0:T(1024)S(1)} %copy-done.2, f32[64]{0:T(128)S(1)} %add_rsqrt_fusion, f32[64]{0:T(128)S(1)} %broadcast_multiply_fusion, f32[4,16,2048]{2,1,0:T(8,128)} %shard_map.182, bf16[64,2048]{1,0:T(8,128)(2,1)S(1)} %copy-done.1), kind=kLoop, calls=%fused_computation.2 | loop fusion | flops 917504 | bytes 1057280 | tf_op jit(solution)/shard_map/convert_element_type | solution.py:1143
  43.1 0.0 copy-done.3
  43.1 0.1 copy.49
  43.2 0.1 eq.63
  43.4 0.1 fusion
  43.5 0.3 reduce_window_sum.11
  43.8 0.2 select_reduce_fusion
  44.0 0.1 copy.50
  44.2 0.1 copy.51
  44.3 0.1 reshape.39
  44.4 0.0 copy-done.4
  44.4 0.7 select_reduce_fusion.1.refs_2_
  45.1 0.8 convert_add_fusion.refs_0_
  45.9 68.9 %shard_map.183 = bf16[64,2048]{1,0:T(8,128)(2,1)} custom-call(f32[4,192,64]{2,1,0:T(8,128)} %convert_add_fusion.refs_0_, bf16[64,2048]{1,0:T(8,128)(2,1)} %multiply_convert_fusion.refs_1_, f32[64,192]{1,0:T(8,128)} %select_reduce_fusion.1.refs_2_, bf16[2,2048,256]{2,1,0:T(8,128)(2,1)} %refs_3_.3, bf16[2,2048,256]{2,1,0:T(8,128)(2,1)} %refs_4_.2, ...), custom_call_target="tpu_custom_call" | custom-call | tf_op jit(solution)/shard_map/pallas_call | solution.py:1063
  114.8 1.7 %copy.55 = bf16[64,2048]{1,0:T(8,128)(2,1)} copy(bf16[64,2048]{1,0:T(8,128)(2,1)} %shard_map.183) | data formatting | bytes 524288
  (6 shorter events, 0.1 us)
Async XLA Ops:
  0.0 23.8 %copy-start = (bf16[512,2048]{1,0:T(8,128)(2,1)S(1)}, bf16[512,2048]{1,0:T(8,128)(2,1)}, u32[]{:S(2)}) copy-start(bf16[512,2048]{1,0:T(8,128)(2,1)} %param.28) | copy-start | bytes 6291460
  23.8 14.9 %copy-start.1 = (bf16[64,2048]{1,0:T(8,128)(2,1)S(1)}, bf16[64,2048]{1,0:T(8,128)(2,1)}, u32[]{:S(2)}) copy-start(bf16[64,2048]{1,0:T(8,128)(2,1)} %param.26) | copy-start | bytes 786436
  26.5 14.7 %copy-start.2 = (f32[2048]{0:T(1024)S(1)}, f32[2048]{0:T(1024)}, u32[]{:S(2)}) copy-start(f32[2048]{0:T(1024)} %param.29) | copy-start | bytes 24580
  26.5 16.6 %copy-start.3 = (s32[256,2]{0,1:T(2,128)S(1)}, s32[256,2]{0,1:T(2,128)}, u32[]{:S(2)}) copy-start(s32[256,2]{0,1:T(2,128)} %param.30) | copy-start | bytes 6148
  38.7 5.7 %copy-start.4 = (f32[64,2]{0,1:T(2,128)S(1)}, f32[64,2]{0,1:T(2,128)}, u32[]{:S(2)}) copy-start(f32[64,2]{0,1:T(2,128)} %param.31) | copy-start | bytes 1540

commit v3 on v2

--- a/solution.py
+++ b/solution.py
@@ -36,22 +36,6 @@
     )
 
 
-def greet(groups):
-    barrier = pltpu.get_barrier_semaphore()
-    count = 0
-    for axis, size in groups:
-        me = lax.axis_index(axis)
-        for step in range(1, size):
-            pl.semaphore_signal(
-                barrier,
-                inc=1,
-                device_id={axis: lax.rem(me + step, size)},
-                device_id_type=MESH,
-            )
-            count += 1
-    pl.semaphore_wait(barrier, count)
-
-
 def chunk_iota(rows, cols, dim):
     return lax.broadcasted_iota(jnp.int32, (rows, cols), dim)
 
@@ -89,8 +73,11 @@
     return top, narrow(values - top.astype(jnp.float32))
 
 
-def mixer_kernel(
+def mixer_body(
     size,
+    sides,
+    block,
+    capacity,
     queries,
     keys,
     values,
@@ -99,8 +86,15 @@
     surges,
     docs,
     scale,
-    out,
-    unit_s,
+    out_weight,
+    residual,
+    layer_scale,
+    routes,
+    route_weight,
+    meet,
+    stream,
+    choice,
+    mix,
     ahead_s,
     fwd_s,
     reads_s,
@@ -120,12 +114,18 @@
     pmap_in,
     s_out,
     s_in,
+    mixed,
+    mixed_near,
+    mixed_pair,
+    mixed_far,
     doc_sem,
     padd_sem,
     pmap_sem,
     near_sem,
     next_sem,
     s_recv,
+    mn_sem,
+    mf_sem,
 ):
     me = lax.axis_index("sp")
     span = BLOCK_SPAN
@@ -133,14 +133,8 @@
     chunks = rows // span
     lanes = 2 * HEAD
     pairs = width // lanes
-    heads = rates.shape[1]
+    heads = rates.shape[0]
     high = lax.Precision.HIGH
-    barrier = pltpu.get_barrier_semaphore()
-    for step in (1, 2, size - 1, size - 2):
-        pl.semaphore_signal(
-            barrier, inc=1, device_id={"sp": lax.rem(me + step, size)}, device_id_type=MESH
-        )
-
     same_half = (chunk_iota(lanes, lanes, 0) // HEAD) == (chunk_iota(lanes, lanes, 1) // HEAD)
     ones_half = same_half.astype(jnp.float32)
     earlier = lax.rem(chunk_iota(span, lanes, 1), HEAD)
@@ -181,7 +175,7 @@
         tail.append((col == doc_col[(c + 1) * span - 1 : (c + 1) * span]).astype(jnp.float32))
 
     doc_out[...] = jnp.broadcast_to(doc_col[rows - 1 : rows], doc_out.shape)
-    pl.semaphore_wait(barrier, 4)
+    meet()
     following = lax.rem(me + 1, size)
     doc_hop = remote(doc_out, doc_in, doc_sem.at[0], doc_sem.at[1], "sp", following)
 
@@ -203,8 +197,8 @@
             key = keys[:, cols].astype(jnp.float32)
             norm = mm(key * key, ones_half, high)
             unit = key * lax.rsqrt(norm + unit_eps)
-            rate = mm(rate_all, spread_heads, high)
-            surge = mm(surge_all, spread_heads, high)
+            rate = mm_tn(rate_all, spread_heads, high)
+            surge = mm_tn(surge_all, spread_heads, high)
             logit = decays[:, cols].astype(jnp.float32)
             decay = surge - jnp.exp(-0.5) / (1.0 + jnp.exp(-logit))
             top, rest = split(decay)
@@ -395,6 +389,49 @@
 
     finish_local()
 
+    own_tp = lax.axis_index("tp")
+    tokens = residual.shape[0]
+    experts = EXP_DEV * size
+    slot_list = size * block
+    named = routes[...].astype(jnp.float32)
+    expert_row = chunk_iota(experts, rows, 0).astype(jnp.float32)
+    taken = jnp.zeros((experts, rows), jnp.float32)
+    for route in range(TOP):
+        taken = taken + (named[route : route + 1] == expert_row).astype(jnp.float32)
+    same_block = (chunk_iota(rows, rows, 0) // tokens) == (chunk_iota(rows, rows, 1) // tokens)
+    prior = ((chunk_iota(rows, rows, 0) < chunk_iota(rows, rows, 1)) & same_block).astype(
+        jnp.bfloat16
+    )
+    taken = narrow(taken)
+    rank = narrow(mm(taken, prior))
+    place = lax.rem(chunk_iota(slot_list, experts, 0), block)
+    hosts = ((chunk_iota(slot_list, experts, 0) // block) * EXP_DEV + place // capacity) == (
+        chunk_iota(slot_list, experts, 1)
+    )
+    hosts = (hosts & (place < EXP_DEV * capacity)).astype(jnp.float32)
+    seat = lax.rem(lax.rem(chunk_iota(slot_list, rows, 0), block), capacity).astype(jnp.float32)
+    chosen = narrow(
+        jnp.where(
+            (mm(narrow(hosts), taken) > 0.5) & (mm(narrow(hosts), rank) == seat), 1.0, 0.0
+        )
+    )
+
+    def part_of(who):
+        return (
+            chunk_iota(rows, tokens, 0) == who * tokens + chunk_iota(rows, tokens, 1)
+        ).astype(jnp.bfloat16)
+
+    for who in range(sides):
+        choice[who] = mm(chosen, part_of(who))
+    named_own = mm(narrow(named), part_of(own_tp))
+    expert_own = chunk_iota(experts, tokens, 0).astype(jnp.float32)
+    amount = jnp.zeros((experts, tokens), jnp.float32)
+    for route in range(TOP):
+        amount = amount + jnp.where(
+            named_own[route : route + 1] == expert_own, route_weight[route : route + 1, :], 0.0
+        )
+    mix[...] = choice[own_tp] * mm(hosts, amount, lax.Precision.HIGHEST)
+
     @pl.when(jnp.logical_not(even))
     def _():
         for p in range(pairs):
@@ -459,13 +496,78 @@
         for p in range(pairs):
             comp_s[p, :HEAD] = s_in[p].astype(jnp.float32)
 
-    for p in range(pairs):
-        cols = slice(p * lanes, (p + 1) * lanes)
-        incoming = narrow(wide(comp_s[p, :HEAD] * join))
-        read = local_s[:, cols] + mm_nt(starts_s[:, cols], incoming)
-        centred = read - mm(read, ones_half, high) * (1.0 / HEAD)
-        spread = mm(centred * centred, ones_half, high) * (1.0 / HEAD)
-        out[:, cols] = narrow(centred * lax.rsqrt(spread + group_eps) * scale[:, cols])
+    half = sides // 2
+    partner = own_tp + 1 - 2 * lax.rem(own_tp, 2)
+    split_rows = 16
+    split_list = tokens // split_rows
+
+    def ahead(j, who=None):
+        return lax.rem((own_tp if who is None else who) + 2 * j, sides)
+
+    def near_hop(j):
+        return remote(
+            mixed.at[ahead(j, partner)], mixed_near.at[j], mn_sem.at[0, j], mn_sem.at[1, j], "tp", partner
+        )
+
+    def far_hop(j, i):
+        span_rows = pl.ds(i * split_rows, split_rows)
+        return remote(
+            mixed_pair.at[j - 1, span_rows],
+            mixed_far.at[j - 1, span_rows],
+            mf_sem.at[0, j, i],
+            mf_sem.at[1, j, i],
+            "tp",
+            ahead(j),
+        )
+
+    incoming = [narrow(wide(comp_s[p, :HEAD] * join)) for p in range(pairs)]
+
+    def project(quarter):
+        part = pl.ds(pl.multiple_of(quarter * tokens, tokens), tokens)
+        normed = []
+        for p in range(pairs):
+            cols = slice(p * lanes, (p + 1) * lanes)
+            read = local_s[part, cols] + mm_nt(starts_s[part, cols], incoming[p])
+            centred = read - mm(read, ones_half, high) * (1.0 / HEAD)
+            spread = mm(centred * centred, ones_half, high) * (1.0 / HEAD)
+            normed.append(
+                narrow(centred * lax.rsqrt(spread + group_eps) * scale[:, cols])
+            )
+        mixed[quarter] = narrow(mm(jnp.concatenate(normed, 1), out_weight[...]))
+
+    for j in range(half - 1, -1, -1):
+        project(ahead(j, partner))
+        near_hop(j).start()
+        project(ahead(j))
+        if j > 0:
+            near_hop(j).wait_recv()
+            for i in range(split_list):
+                take = slice(i * split_rows, (i + 1) * split_rows)
+                mixed_pair[j - 1, take] = narrow(
+                    mixed[ahead(j), take].astype(jnp.float32)
+                    + mixed_near[j, take].astype(jnp.float32)
+                )
+                far_hop(j, i).start()
+    near_hop(0).wait_recv()
+    for i in range(split_list):
+        take = slice(i * split_rows, (i + 1) * split_rows)
+        total = (
+            residual_scale * residual[take].astype(jnp.float32)
+            + mixed[own_tp, take].astype(jnp.float32)
+            + mixed_near[0, take].astype(jnp.float32)
+        )
+        for j in range(1, half):
+            far_hop(j, i).wait_recv()
+            total = total + mixed_far[j - 1, take].astype(jnp.float32)
+        centred = total - jnp.mean(total, -1, keepdims=True)
+        spread = jnp.mean(centred * centred, -1, keepdims=True)
+        stream[take] = narrow(centred * lax.rsqrt(spread + norm_eps) * layer_scale[...])
+
+    for j in range(half):
+        near_hop(j).wait_send()
+        if j > 0:
+            for i in range(split_list):
+                far_hop(j, i).wait_send()
 
     @pl.when(me < size - 1)
     def _():
@@ -482,180 +584,6 @@
         for p in range(pairs):
             state_hop(p, True).wait_send()
             state_hop(p, False).wait_send()
-
-
-def mixer(queries, keys, values, decays, rates, surges, documents, scale):
-    size = lax.axis_size("sp")
-    rows, width = queries.shape
-    lanes = 2 * HEAD
-    pairs = width // lanes
-    chunks = rows // BLOCK_SPAN
-    f32, b16 = jnp.float32, jnp.bfloat16
-    dma = pltpu.SemaphoreType.DMA
-    return pl.pallas_call(
-        lambda *refs: mixer_kernel(size, *refs),
-        out_shape=jax.ShapeDtypeStruct((rows, width), b16),
-        in_specs=[VMEM] * 8,
-        out_specs=VMEM,
-        scratch_shapes=[
-            pltpu.VMEM((8, lanes), f32),
-            pltpu.VMEM((rows, width), f32),
-            pltpu.VMEM((rows, width), f32),
-            pltpu.VMEM((chunks, pairs, BLOCK_SPAN, 2 * lanes), b16),
-            pltpu.VMEM((chunks, pairs, BLOCK_SPAN, 2 * lanes), b16),
-            pltpu.VMEM((chunks, pairs, lanes, lanes), f32),
-            pltpu.VMEM((chunks, pairs, HEAD, lanes), f32),
-            pltpu.VMEM((rows, width), f32),
-            pltpu.VMEM((rows, width), b16),
-            pltpu.VMEM((pairs, lanes, lanes), f32),
-            pltpu.VMEM((pairs, lanes, lanes), f32),
-            pltpu.VMEM((8, lanes), f32),
-            pltpu.VMEM((8, lanes), f32),
-            pltpu.VMEM((8, lanes), f32),
-            pltpu.VMEM((pairs, HEAD, lanes), b16),
-            pltpu.VMEM((pairs, HEAD, lanes), b16),
-            pltpu.VMEM((pairs, HEAD, lanes), f32),
-            pltpu.VMEM((pairs, HEAD, lanes), f32),
-            pltpu.VMEM((pairs, HEAD, lanes), b16),
-            pltpu.VMEM((pairs, HEAD, lanes), b16),
-            dma((2,)),
-            dma((2, pairs)),
-            dma((2, pairs)),
-            dma((pairs,)),
-            dma((pairs,)),
-            dma((pairs,)),
-        ],
-        compiler_params=pltpu.CompilerParams(collective_id=1, has_side_effects=True),
-    )(
-        queries,
-        keys,
-        values,
-        decays,
-        rates,
-        surges,
-        documents.reshape(1, rows),
-        scale.reshape(1, width),
-    )
-
-
-def tp_reduce_kernel(size, groups, sends_back, *refs):
-    if sends_back:
-        (parts, extra, out, extra_out, near, pair, far, enear, epair, efar, stage) = refs[:11]
-        sems = refs[11:]
-    else:
-        (parts, out, near, pair, far) = refs[:5]
-        sems = refs[5:]
-    nsend, nrecv, fsend, frecv = sems[:4]
-    me = lax.axis_index("tp")
-    own = lax.axis_index("sp")
-    half = size // 2
-    partner = me + 1 - 2 * lax.rem(me, 2)
-    pieces = parts.shape[1]
-    greet((("tp", size), ("sp", groups)) if sends_back else (("tp", size),))
-
-    jobs = []
-    for step in range(pieces):
-        where = lax.rem(own + 1 + step, pieces) if sends_back else step
-        jobs.append((step, parts, near, pair, far, where))
-    if sends_back:
-        jobs.append((pieces, extra, enear, epair, efar, 0))
-
-    def near_copy(job, k):
-        slot, src, to, _, _, where = job
-        return remote(
-            src.at[lax.rem(partner + 2 * k, size), where],
-            to.at[k, where],
-            nsend.at[slot, k],
-            nrecv.at[slot, k],
-            "tp",
-            partner,
-        )
-
-    def far_copy(job, k):
-        slot, _, _, src, to, where = job
-        return remote(
-            src.at[k - 1, where],
-            to.at[k - 1, where],
-            fsend.at[slot, k],
-            frecv.at[slot, k],
-            "tp",
-            lax.rem(me + 2 * k, size),
-        )
-
-    for job in jobs:
-        for k in range(half - 1, -1, -1):
-            near_copy(job, k).start()
-
-    def add_pair(job):
-        slot, src, to, mid, _, where = job
-        for k in range(1, half):
-            near_copy(job, k).wait_recv()
-            mid[k - 1, where] = (
-                src[lax.rem(me + 2 * k, size), where].astype(jnp.float32)
-                + to[k, where].astype(jnp.float32)
-            ).astype(jnp.bfloat16)
-            far_copy(job, k).start()
-
-    def back_copy(step):
-        target = lax.rem(own + 1 + step, pieces)
-        return remote(
-            stage.at[target], out.at[own], sems[4].at[step], sems[5].at[step], "sp", target
-        )
-
-    def finish(job):
-        slot, src, to, _, last, where = job
-        near_copy(job, 0).wait_recv()
-        total = src[me, where].astype(jnp.float32) + to[0, where].astype(jnp.float32)
-        for k in range(1, half):
-            far_copy(job, k).wait_recv()
-            total = total + last[k - 1, where].astype(jnp.float32)
-        if not sends_back:
-            out[where] = total
-        elif slot == pieces:
-            extra_out[...] = total
-        elif slot == pieces - 1:
-            out[own] = total.astype(jnp.bfloat16)
-        else:
-            stage[where] = total.astype(jnp.bfloat16)
-            back_copy(slot).start()
-
-    lag = 2
-    for turn in range(len(jobs) + lag):
-        if turn < len(jobs):
-            add_pair(jobs[turn])
-        if turn >= lag:
-            finish(jobs[turn - lag])
-    for job in jobs:
-        for k in range(half):
-            near_copy(job, k).wait_send()
-        for k in range(1, half):
-            far_copy(job, k).wait_send()
-    if sends_back:
-        for step in range(pieces - 1):
-            back_copy(step).wait_send()
-            sender = lax.rem(own - 1 - step + pieces, pieces)
-            remote(
-                stage.at[sender], out.at[sender], sems[4].at[step], sems[5].at[step], "sp", sender
-            ).wait_recv()
-
-
-def tp_reduce(parts):
-    size, pieces, rows, width = parts.shape
-    half = size // 2
-    kind = jnp.bfloat16
-    return pl.pallas_call(
-        lambda *refs: tp_reduce_kernel(size, 1, False, *refs),
-        out_shape=jax.ShapeDtypeStruct((pieces, rows, width), jnp.float32),
-        in_specs=[VMEM],
-        out_specs=VMEM,
-        scratch_shapes=[
-            pltpu.VMEM((half, pieces, rows, width), kind),
-            pltpu.VMEM((half - 1, pieces, rows, width), kind),
-            pltpu.VMEM((half - 1, pieces, rows, width), kind),
-        ]
-        + [pltpu.SemaphoreType.DMA((pieces, half))] * 4,
-        compiler_params=pltpu.CompilerParams(collective_id=2, has_side_effects=True),
-    )(parts)
 
 
 def flip(index, bits, size):
@@ -667,25 +595,20 @@
     return total
 
 
-def moe_kernel(
+def moe_body(
     size,
     groups,
     capacity,
     block,
+    fetches,
     choice,
     stream,
     mix,
-    gate,
-    upward,
-    down,
-    common_gate,
-    common_up,
-    common_down,
     out,
     outgoing,
     near_out,
+    returned_far,
     mix_far,
-    returned_far,
     stage_far,
     arrived,
     rows_all,
@@ -699,14 +622,13 @@
     enear,
     epair,
     efar,
+    cgate_v,
+    cup_v,
+    cdown_v,
     gate_v,
     up_v,
     down_v,
-    cgate_v,
-    cup_v,
-    cdown_v,
     local,
-    loads,
     asend,
     arecv,
     nsend,
@@ -732,27 +654,9 @@
     close = min(CLOSE, groups)
     batch = max(1, groups // 8)
     steps = groups // batch
-    fetches = [
-        pltpu.make_async_copy(src, dst, loads.at[i])
-        for i, (src, dst) in enumerate(
-            (
-                (common_gate, cgate_v),
-                (common_up, cup_v),
-                (common_down, cdown_v),
-                (gate, gate_v),
-                (upward, up_v),
-                (down, down_v),
-            )
-        )
-    ]
-    for fetch in fetches:
-        fetch.start()
     keep_rows = pltpu.make_async_copy(stream, rows_all.at[me], local.at[1])
     keep_rows.start()
-    returned_far[...] = jnp.zeros_like(returned_far)
     outgoing[...] = narrow(mm(narrow(choice[me]), stream[...])).reshape(groups, block, width)
-    greet((("tp", size), ("sp", groups)))
-
     def ahead(j):
         return lax.rem(me + 2 * j, size)
 
@@ -863,7 +767,7 @@
     def weighed(weights, rows):
         top, rest = split(weights)
         rows = narrow(rows.astype(jnp.float32).reshape(groups * block, width))
-        return mm(top, rows) + mm(rest, rows)
+        return mm_tn(top, rows) + mm_tn(rest, rows)
 
     def add_extra():
         for k in range(1, close):
@@ -1048,52 +952,166 @@
         send_mix(j).wait_send()
 
 
-def moe(
-    choice, stream, mix, gate, upward, down, common_gate, common_up, common_down, capacity, block
-):
-    size = lax.axis_size("tp")
+def layer_kernel(size, sides, block, capacity, counts, *refs):
+    refs = list(refs)
+
+    def take(count):
+        got = refs[:count]
+        del refs[:count]
+        return got
+
+    mixer_in = take(12)
+    big = take(7)
+    (out,) = take(1)
+    big_v = take(7)
+    (loads,) = take(1)
+    meeting = take(3)
+    mixer_scratch = take(counts[0])
+    moe_scratch = take(counts[1])
+    returned_far = moe_scratch[2]
+    fetches = [
+        pltpu.make_async_copy(src, dst, loads.at[i]) for i, (src, dst) in enumerate(zip(big, big_v))
+    ]
+    for fetch in fetches:
+        fetch.start()
+    returned_far[...] = jnp.zeros_like(returned_far)
+    barrier = pltpu.get_barrier_semaphore()
+    peers = 0
+    for axis, number in (("sp", size), ("tp", sides)):
+        here = lax.axis_index(axis)
+        for step in range(1, number):
+            pl.semaphore_signal(
+                barrier,
+                inc=1,
+                device_id={axis: lax.rem(here + step, number)},
+                device_id_type=MESH,
+            )
+            peers += 1
+
+    def meet():
+        pl.semaphore_wait(barrier, peers)
+        fetches[0].wait()
+
+    stream, choice, mix = meeting
+    mixer_body(
+        size,
+        sides,
+        block,
+        capacity,
+        *mixer_in[:8],
+        big_v[0],
+        *mixer_in[8:],
+        meet,
+        stream,
+        choice,
+        mix,
+        *mixer_scratch,
+    )
+    moe_body(
+        sides,
+        size,
+        capacity,
+        block,
+        fetches[1:],
+        choice,
+        stream,
+        mix,
+        out,
+        *moe_scratch[:-17],
+        *big_v[1:],
+        *moe_scratch[-17:],
+    )
+
+
+def layer(mixer_in, big, block, capacity):
+    sides = lax.axis_size("tp")
     groups = lax.axis_size("sp")
-    tokens, width = stream.shape
+    rows, width_in = mixer_in[0].shape
+    tokens, width = mixer_in[8].shape
+    lanes = 2 * HEAD
+    pairs = width_in // lanes
+    chunks = rows // BLOCK_SPAN
     close = min(CLOSE, groups)
-    half = size // 2
+    half = sides // 2
+    f32, b16 = jnp.float32, jnp.bfloat16
     dma = pltpu.SemaphoreType.DMA
-    b16, f32 = jnp.bfloat16, jnp.float32
+    vmem = pltpu.VMEM
     anywhere = pl.BlockSpec(memory_space=pl.ANY)
-    weights = (gate, upward, down, common_gate, common_up, common_down)
-    return pl.pallas_call(
-        lambda *refs: moe_kernel(size, groups, capacity, block, *refs),
-        out_shape=jax.ShapeDtypeStruct((tokens, width), b16),
-        in_specs=[VMEM] * 3 + [anywhere] * 6,
-        out_specs=VMEM,
-        scratch_shapes=[
-            pltpu.VMEM((groups, block, width), b16),
-            pltpu.VMEM((close, half, block, width), b16),
-            pltpu.VMEM((half - 1,) + mix.shape, f32),
-            pltpu.VMEM((half - 1, groups, block, width), b16),
-            pltpu.VMEM((half - 1, close, block, width), b16),
-            pltpu.VMEM((size, groups, block, width), b16),
-            pltpu.VMEM((size, tokens, width), b16),
-            pltpu.VMEM((size, groups, block, width), b16),
-            pltpu.VMEM((half, groups, block, width), b16),
-            pltpu.VMEM((half - 1, groups, block, width), b16),
-            pltpu.VMEM((half - 1, groups, block, width), b16),
-            pltpu.VMEM((groups, block, width), b16),
-            pltpu.VMEM((groups, block, width), b16),
-            pltpu.VMEM((size, 1, tokens, width), b16),
-            pltpu.VMEM((half, 1, tokens, width), b16),
-            pltpu.VMEM((half - 1, 1, tokens, width), b16),
-            pltpu.VMEM((half - 1, 1, tokens, width), b16),
+    slots = groups * block
+    mixer_scratch = [
+        vmem((rows, width_in), f32),
+        vmem((rows, width_in), f32),
+        vmem((chunks, pairs, BLOCK_SPAN, 2 * lanes), b16),
+        vmem((chunks, pairs, BLOCK_SPAN, 2 * lanes), b16),
+        vmem((chunks, pairs, lanes, lanes), f32),
+        vmem((chunks, pairs, HEAD, lanes), f32),
+        vmem((rows, width_in), f32),
+        vmem((rows, width_in), b16),
+        vmem((pairs, lanes, lanes), f32),
+        vmem((pairs, lanes, lanes), f32),
+        vmem((8, lanes), f32),
+        vmem((8, lanes), f32),
+        vmem((8, lanes), f32),
+        vmem((pairs, HEAD, lanes), b16),
+        vmem((pairs, HEAD, lanes), b16),
+        vmem((pairs, HEAD, lanes), f32),
+        vmem((pairs, HEAD, lanes), f32),
+        vmem((pairs, HEAD, lanes), b16),
+        vmem((pairs, HEAD, lanes), b16),
+        vmem((sides, tokens, width), b16),
+        vmem((half, tokens, width), b16),
+        vmem((half - 1, tokens, width), b16),
+        vmem((half - 1, tokens, width), b16),
+        dma((2,)),
+        dma((2, pairs)),
+        dma((2, pairs)),
+        dma((pairs,)),
+        dma((pairs,)),
+        dma((pairs,)),
+        dma((2, half)),
+        dma((2, half, tokens // 16)),
+    ]
+    moe_scratch = (
+        [
+            vmem((groups, block, width), b16),
+            vmem((close, half, block, width), b16),
+            vmem((half - 1, groups, block, width), b16),
+            vmem((half - 1, slots, tokens), f32),
+            vmem((half - 1, close, block, width), b16),
+            vmem((sides, groups, block, width), b16),
+            vmem((sides, tokens, width), b16),
+            vmem((sides, groups, block, width), b16),
+            vmem((half, groups, block, width), b16),
+            vmem((half - 1, groups, block, width), b16),
+            vmem((half - 1, groups, block, width), b16),
+            vmem((groups, block, width), b16),
+            vmem((groups, block, width), b16),
+            vmem((sides, 1, tokens, width), b16),
+            vmem((half, 1, tokens, width), b16),
+            vmem((half - 1, 1, tokens, width), b16),
+            vmem((half - 1, 1, tokens, width), b16),
         ]
-        + [pltpu.VMEM(w.shape, b16) for w in weights]
-        + [dma((2,)), dma((6,)), dma((groups, half)), dma((groups, half))]
+        + [dma((2,)), dma((groups, half)), dma((groups, half))]
         + [dma((groups + 1,))] * 2
         + [dma((groups + 1, half))] * 8
         + [dma((groups, half))] * 2
-        + [dma((half,))] * 2,
+        + [dma((half,))] * 2
+    )
+    counts = (len(mixer_scratch), len(moe_scratch))
+    return pl.pallas_call(
+        lambda *refs: layer_kernel(groups, sides, block, capacity, counts, *refs),
+        out_shape=jax.ShapeDtypeStruct((tokens, width), b16),
+        in_specs=[VMEM] * 12 + [anywhere] * 7,
+        out_specs=VMEM,
+        scratch_shapes=[vmem(w.shape, b16) for w in big]
+        + [dma((7,))]
+        + [vmem((tokens, width), b16), vmem((sides, slots, tokens), f32), vmem((slots, tokens), f32)]
+        + mixer_scratch
+        + moe_scratch,
         compiler_params=pltpu.CompilerParams(
-            collective_id=4, has_side_effects=True, vmem_limit_bytes=60 * 1024 * 1024
+            collective_id=1, has_side_effects=True, vmem_limit_bytes=67_000_000
         ),
-    )(choice, stream, mix, *weights)
+    )(*mixer_in, *big)
 
 
 def per_device(
@@ -1117,62 +1135,34 @@
     common_up_weight,
     common_down_weight,
 ):
-    head_outputs = mixer(
+    groups = lax.axis_size("sp")
+    experts = EXP_DEV * groups
+    capacity = max(2, (3 * TOK_DEV * TOP + 2 * experts - 1) // (2 * experts))
+    block_rows = 8 * ((EXP_DEV * capacity + 7) // 8)
+    mixer_in = (
         head_queries,
         head_keys,
         head_values,
         decay_logits,
-        learning_logits,
-        surge_decay,
-        documents,
-        head_norm_scale,
-    )
-    quarters = lax.axis_size("tp")
-    groups = lax.axis_size("sp")
-    own_rows, model_width = residual.shape
-    pieces = own_rows // 16
-    mixed_parts = jnp.dot(
-        head_outputs, mixer_output_weight, preferred_element_type=jnp.float32
-    ).astype(jnp.bfloat16)
-    mixed_rows = tp_reduce(mixed_parts.reshape(quarters, pieces, 16, model_width)).reshape(
-        own_rows, model_width
-    )
-    summed = residual_scale * residual.astype(jnp.float32) + mixed_rows
-    centre = jnp.mean(summed, -1, keepdims=True)
-    spread = jnp.mean(jnp.square(summed - centre), -1, keepdims=True)
-    stream = ((summed - centre) * lax.rsqrt(spread + norm_eps) * layer_norm_scale).astype(
-        jnp.bfloat16
-    )
-    experts = EXP_DEV * groups
-    capacity = max(2, (3 * TOK_DEV * TOP + 2 * experts - 1) // (2 * experts))
-    block_rows = 8 * ((EXP_DEV * capacity + 7) // 8)
-    chosen = routes.reshape(quarters, own_rows * TOP)
-    onehot = (chosen[..., None] == jnp.arange(experts, dtype=jnp.int32)).astype(jnp.int32)
-    ranking = jnp.sum(jnp.cumsum(onehot, 1) * onehot, -1) - 1
-    slot_index = (
-        chosen // EXP_DEV * block_rows + chosen % EXP_DEV * capacity + ranking
-    )
-    slot_index = slot_index.reshape(quarters, own_rows, TOP)
-    own_slots = lax.dynamic_index_in_dim(slot_index, lax.axis_index("tp"), 0, keepdims=False)
-    slots = jnp.arange(groups * block_rows, dtype=jnp.int32)
-    hits = own_slots[:, :, None] == slots
-    choice = jnp.zeros((quarters, groups * block_rows, own_rows), jnp.float32)
-    for route in range(TOP):
-        choice = choice + (slots[None, :, None] == slot_index[:, None, :, route])
-    weights = jnp.sum(jnp.where(hits, routing_weight[:, :, None], 0.0), 1)
-    return moe(
-        choice,
-        stream,
-        weights,
+        learning_logits.T,
+        surge_decay.T,
+        documents.reshape(1, -1),
+        head_norm_scale.reshape(1, -1),
+        residual,
+        layer_norm_scale.reshape(1, -1),
+        routes.T,
+        routing_weight.T,
+    )
+    big = (
+        mixer_output_weight,
+        common_gate_weight,
+        common_up_weight,
+        common_down_weight,
         routed_gate_weight,
         routed_up_weight,
         routed_down_weight,
-        common_gate_weight,
-        common_up_weight,
-        common_down_weight,
-        capacity,
-        block_rows,
-    )
+    )
+    return layer(mixer_in, big, block_rows, capacity)
 
 
 def solution(mesh):

time: 117 us -> 96.9 us (0.83)
  Pallas kernels: 102 us -> 95 us
  other arithmetic: 6.58 us -> 0 us
  local copies, waits for them, and re-layouts: 5.31 us -> 1.67 us
  matrix products: 2.7 us -> 0 us
    pallas_call x3 -> x1, Pallas kernels: 102 us -> 95 us  [layer(): pl.pallas_call(lambda *refs: layer_kernel(groups, sides, block, capacity,...]
    reduce_sum x4 -> x0, other arithmetic: 3.45 us -> none  [the longest x1 1.27 us: per_device(): spread = jnp.mean(jnp.square(summed - centre), -1, keepdims=True)]
    unnamed x14 -> x1, local copies, waits for them, and re-layouts: 4.87 us -> 1.67 us
    dot_general x1 -> x0, matrix products: 2.7 us -> none  [per_device(): jnp.dot(head_outputs, mixer_output_weight, preferred_element_type=jnp.flo...]
    convert_element_type x2 -> x0, other arithmetic: 2.02 us -> none  [the longest x1 1.88 us: per_device(): ((summed - centre) * lax.rsqrt(spread + norm_eps) * layer_norm_scale).ast...]
where the time goes in v3:
time: 96.9 us; the launch traced here: 96.7 us
  Pallas kernels  95 us (98%)
  local copies, waits for them, and re-layouts  1.67 us (2%)
    pallas_call x1, Pallas kernels, layer(): pl.pallas_call(lambda *refs: layer_kernel(groups, sides, block, capacity,...  95 us

profile of v3, /device:TPU:0, one launch (start us, length us, event | category | flops | bytes accessed | tf_op | source)
XLA Modules:
  0.0 96.7 jit_solution(12595450485535313600)
XLA Ops:
  0.0 95.0 %shard_map.181 = bf16[64,2048]{1,0:T(8,128)(2,1)} custom-call(bf16[256,512]{1,0:T(8,128)(2,1)} %refs_0_.1, bf16[256,512]{1,0:T(8,128)(2,1)} %refs_1_.1, bf16[256,512]{1,0:T(8,128)(2,1)} %refs_2_.1, bf16[256,512]{1,0:T(8,128)(2,1)} %refs_3_.1, bf16[8,256]{1,0:T(8,128)(2,1)} %bitcast.9, f32[8,256]{1,0:T(8,128)} %bitcast.7, s32[1,256]{1,0:T(1,128)} %bitcast.12, ...), custom_call_target="tpu_custom_call" | custom-call | tf_op jit(solution)/shard_map/pallas_call | solution.py:1101
  95.0 1.7 %copy.21 = bf16[64,2048]{1,0:T(8,128)(2,1)} copy(bf16[64,2048]{1,0:T(8,128)(2,1)} %shard_map.181) | data formatting | bytes 524288

commit v4 on v3

--- a/solution.py
+++ b/solution.py
@@ -16,9 +16,10 @@
 group_eps = 0.00064
 norm_eps = 1e-05
 unit_eps = 1e-06
-CLOSE = 2
-EXTRA_TURN = 5
-SCORE_PRECISION = lax.Precision.HIGH
+CLOSE_PLACE = 3
+EXTRA_TURN = 8
+NEAR_TURN = 1
+LEAD = 5
 
 
 MESH = pl.DeviceIdType.MESH
@@ -71,6 +72,51 @@
 def split(values):
     top = narrow(values)
     return top, narrow(values - top.astype(jnp.float32))
+
+
+def assign_slots(
+    size, sides, block, capacity, rows, tokens, own_tp, routes, route_weight, choice, mix
+):
+    experts = EXP_DEV * size
+    slot_list = size * block
+    named = routes[...].astype(jnp.float32)
+    expert_row = chunk_iota(experts, rows, 0).astype(jnp.float32)
+    taken = jnp.zeros((experts, rows), jnp.float32)
+    for route in range(TOP):
+        taken = taken + (named[route : route + 1] == expert_row).astype(jnp.float32)
+    same_block = (chunk_iota(rows, rows, 0) // tokens) == (chunk_iota(rows, rows, 1) // tokens)
+    prior = ((chunk_iota(rows, rows, 0) < chunk_iota(rows, rows, 1)) & same_block).astype(
+        jnp.bfloat16
+    )
+    taken = narrow(taken)
+    rank = narrow(mm(taken, prior))
+    place = lax.rem(chunk_iota(slot_list, experts, 0), block)
+    hosts = ((chunk_iota(slot_list, experts, 0) // block) * EXP_DEV + place // capacity) == (
+        chunk_iota(slot_list, experts, 1)
+    )
+    hosts = (hosts & (place < EXP_DEV * capacity)).astype(jnp.float32)
+    seat = lax.rem(lax.rem(chunk_iota(slot_list, rows, 0), block), capacity).astype(jnp.float32)
+    chosen = narrow(
+        jnp.where(
+            (mm(narrow(hosts), taken) > 0.5) & (mm(narrow(hosts), rank) == seat), 1.0, 0.0
+        )
+    )
+
+    def part_of(who):
+        return (
+            chunk_iota(rows, tokens, 0) == who * tokens + chunk_iota(rows, tokens, 1)
+        ).astype(jnp.bfloat16)
+
+    for who in range(sides):
+        choice[who] = mm(chosen, part_of(who))
+    named_own = mm(narrow(named), part_of(own_tp))
+    expert_own = chunk_iota(experts, tokens, 0).astype(jnp.float32)
+    amount = jnp.zeros((experts, tokens), jnp.float32)
+    for route in range(TOP):
+        amount = amount + jnp.where(
+            named_own[route : route + 1] == expert_own, route_weight[route : route + 1, :], 0.0
+        )
+    mix[...] = choice[own_tp] * mm(hosts, amount, lax.Precision.HIGHEST)
 
 
 def mixer_body(
@@ -236,7 +282,7 @@
             scores = mm_nt(
                 jnp.concatenate([s["ahead"], s["fwd"]], 0),
                 jnp.concatenate([wide(s["bu"]), wide(s["bk"])], 0),
-                SCORE_PRECISION,
+                high,
             )
             s["low"] = jnp.where(strict[c], scores[:span, :lanes], 0.0)
             s["mixk"] = jnp.where(strict[c], scores[:span, lanes:], 0.0)
@@ -387,50 +433,18 @@
                 local_s[part, cols] = local
                 starts_s[part, cols] = narrow(start)
 
-    finish_local()
-
     own_tp = lax.axis_index("tp")
     tokens = residual.shape[0]
-    experts = EXP_DEV * size
-    slot_list = size * block
-    named = routes[...].astype(jnp.float32)
-    expert_row = chunk_iota(experts, rows, 0).astype(jnp.float32)
-    taken = jnp.zeros((experts, rows), jnp.float32)
-    for route in range(TOP):
-        taken = taken + (named[route : route + 1] == expert_row).astype(jnp.float32)
-    same_block = (chunk_iota(rows, rows, 0) // tokens) == (chunk_iota(rows, rows, 1) // tokens)
-    prior = ((chunk_iota(rows, rows, 0) < chunk_iota(rows, rows, 1)) & same_block).astype(
-        jnp.bfloat16
-    )
-    taken = narrow(taken)
-    rank = narrow(mm(taken, prior))
-    place = lax.rem(chunk_iota(slot_list, experts, 0), block)
-    hosts = ((chunk_iota(slot_list, experts, 0) // block) * EXP_DEV + place // capacity) == (
-        chunk_iota(slot_list, experts, 1)
-    )
-    hosts = (hosts & (place < EXP_DEV * capacity)).astype(jnp.float32)
-    seat = lax.rem(lax.rem(chunk_iota(slot_list, rows, 0), block), capacity).astype(jnp.float32)
-    chosen = narrow(
-        jnp.where(
-            (mm(narrow(hosts), taken) > 0.5) & (mm(narrow(hosts), rank) == seat), 1.0, 0.0
+
+    def assign():
+        assign_slots(
+            size, sides, block, capacity, rows, tokens, own_tp, routes, route_weight, choice, mix
         )
-    )
-
-    def part_of(who):
-        return (
-            chunk_iota(rows, tokens, 0) == who * tokens + chunk_iota(rows, tokens, 1)
-        ).astype(jnp.bfloat16)
-
-    for who in range(sides):
-        choice[who] = mm(chosen, part_of(who))
-    named_own = mm(narrow(named), part_of(own_tp))
-    expert_own = chunk_iota(experts, tokens, 0).astype(jnp.float32)
-    amount = jnp.zeros((experts, tokens), jnp.float32)
-    for route in range(TOP):
-        amount = amount + jnp.where(
-            named_own[route : route + 1] == expert_own, route_weight[route : route + 1, :], 0.0
-        )
-    mix[...] = choice[own_tp] * mm(hosts, amount, lax.Precision.HIGHEST)
+
+    @pl.when(even)
+    def _():
+        finish_local()
+        assign()
 
     @pl.when(jnp.logical_not(even))
     def _():
@@ -449,6 +463,13 @@
             for p in range(pairs):
                 s_out[p] = narrow(far_s[p, :HEAD])
                 state_hop(p, True).start()
+                state_hop(p, False).start()
+
+        finish_local()
+
+        @pl.when((me == 1) | (me > 3))
+        def _():
+            assign()
 
         for p in range(pairs):
             pair_hop(p)[1].wait_recv()
@@ -473,10 +494,14 @@
                     )
                     state_hop(p, True).start()
 
-        @pl.when(me < size - 1)
-        def _():
-            for p in range(pairs):
-                state_hop(p, False).start()
+            @pl.when(me < size - 1)
+            def _():
+                for p in range(pairs):
+                    state_hop(p, False).start()
+
+            @pl.when(me == 3)
+            def _():
+                assign()
 
         for p in range(pairs):
             top, rest = split(wide(pmap_in[p]))
@@ -522,23 +547,26 @@
 
     incoming = [narrow(wide(comp_s[p, :HEAD] * join)) for p in range(pairs)]
 
-    def project(quarter):
-        part = pl.ds(pl.multiple_of(quarter * tokens, tokens), tokens)
+    def project(quarters):
+        parts = [pl.ds(pl.multiple_of(q * tokens, tokens), tokens) for q in quarters]
         normed = []
         for p in range(pairs):
             cols = slice(p * lanes, (p + 1) * lanes)
-            read = local_s[part, cols] + mm_nt(starts_s[part, cols], incoming[p])
+            read = jnp.concatenate([local_s[part, cols] for part in parts], 0) + mm_nt(
+                jnp.concatenate([starts_s[part, cols] for part in parts], 0), incoming[p]
+            )
             centred = read - mm(read, ones_half, high) * (1.0 / HEAD)
             spread = mm(centred * centred, ones_half, high) * (1.0 / HEAD)
             normed.append(
                 narrow(centred * lax.rsqrt(spread + group_eps) * scale[:, cols])
             )
-        mixed[quarter] = narrow(mm(jnp.concatenate(normed, 1), out_weight[...]))
+        product = narrow(mm(jnp.concatenate(normed, 1), out_weight[...]))
+        for i, quarter in enumerate(quarters):
+            mixed[quarter] = product[i * tokens : (i + 1) * tokens]
 
     for j in range(half - 1, -1, -1):
-        project(ahead(j, partner))
+        project([ahead(j, partner), ahead(j)])
         near_hop(j).start()
-        project(ahead(j))
         if j > 0:
             near_hop(j).wait_recv()
             for i in range(split_list):
@@ -593,6 +621,12 @@
         total = total + lax.rem(lax.div(index, place) + lax.div(bits, place), 2) * place
         place = place * 2
     return total
+
+
+def piece(position, groups):
+    later = lax.div(lax.div(position, 4) + groups, groups + 1)
+    early = (1 + lax.rem(position, 3)) * lax.div(position + 3, 4)
+    return later * position + (1 - later) * early
 
 
 def moe_body(
@@ -651,19 +685,17 @@
     half = size // 2
     partner = me + 1 - 2 * lax.rem(me, 2)
     tokens, width = stream.shape
-    close = min(CLOSE, groups)
     batch = max(1, groups // 8)
     steps = groups // batch
     keep_rows = pltpu.make_async_copy(stream, rows_all.at[me], local.at[1])
     keep_rows.start()
-    outgoing[...] = narrow(mm(narrow(choice[me]), stream[...])).reshape(groups, block, width)
     def ahead(j):
         return lax.rem(me + 2 * j, size)
 
     def exchange(k, j=0, near=False):
-        other = flip(own, k, groups)
+        other = flip(own, piece(k, groups), groups)
         return remote(
-            near_out.at[k, j] if near else outgoing.at[other],
+            near_out.at[j] if near else outgoing.at[other],
             arrived.at[ahead(j), k],
             asend.at[k, j],
             arecv.at[k, j],
@@ -731,10 +763,10 @@
         )
 
     def back(k, j=0, whose=None):
-        other = flip(own, k, groups)
+        other = flip(own, piece(k, groups), groups)
         where = own if whose is None else whose
         return remote(
-            stage.at[k] if j == 0 else stage_far.at[j - 1, k],
+            stage.at[k] if j == 0 else stage_far.at[j - 1],
             returned.at[where] if j == 0 else returned_far.at[j - 1, where],
             bsend.at[k, j],
             brecv.at[k, j],
@@ -761,7 +793,7 @@
                 if j == 0:
                     stage[k] = total
                 else:
-                    stage_far[j - 1, k] = total
+                    stage_far[j - 1] = total
                 back(k, j).start()
 
     def weighed(weights, rows):
@@ -770,9 +802,9 @@
         return mm_tn(top, rows) + mm_tn(rest, rows)
 
     def add_extra():
-        for k in range(1, close):
-            for j in range(half):
-                back(k, j, flip(own, k, groups)).wait_recv()
+        k = CLOSE_PLACE
+        for j in range(half):
+            back(k, j, flip(own, piece(k, groups), groups)).wait_recv()
         for j in range(1, half):
             reduce_near(groups, j, True).wait_recv()
             send_mix(j).wait_recv()
@@ -811,23 +843,30 @@
     def swish(gated, lifted):
         return gated / (1.0 + jnp.exp(-gated)) * lifted
 
-    lead, relay = min(4, steps), min(2, steps)
+    lead, relay = min(LEAD, steps), min(2, steps)
+
+    def send_pieces(low, high):
+        for k in range(max(1, low), min(high, groups)):
+            if k != CLOSE_PLACE:
+                exchange(k).wait_recv()
+                send_own(k)
+
     send_own(groups, True)
-    for k in range(close, groups):
-        exchange(k).start()
+    outgoing[...] = narrow(mm(narrow(choice[me]), stream[...])).reshape(groups, block, width)
+    for k in range(1, groups):
+        if k != CLOSE_PLACE:
+            exchange(k).start()
     for j in range(1, half):
         send_mix(j).start()
+    send_pieces(1, 4 * batch)
     keep_rows.wait()
     pass_on(groups, True)
-    for k in range(1, close):
-        other = flip(own, k, groups)
-        for j in range(half):
-            picked = narrow(choice[ahead(j), pl.ds(pl.multiple_of(other * block, 8), block)])
-            near_out[k, j] = narrow(mm(picked, rows_all[ahead(j)]))
-            exchange(k, j, True).start()
-    for k in range(close, lead * batch):
-        exchange(k).wait_recv()
-        send_own(k)
+    other = flip(own, piece(CLOSE_PLACE, groups), groups)
+    for j in range(half):
+        picked = narrow(choice[ahead(j), pl.ds(pl.multiple_of(other * block, 8), block)])
+        near_out[j] = narrow(mm(picked, rows_all[ahead(j)]))
+        exchange(CLOSE_PLACE, j, True).start()
+    send_pieces(4 * batch, 5 * batch)
     gathered(groups, True)
     for who in range(size):
         picked = narrow(choice[who, pl.ds(pl.multiple_of(own * block, 8), block)])
@@ -836,18 +875,25 @@
         fetch.wait()
     everyone = rows_all[...].reshape(size * tokens, width)
     hidden = narrow(swish(mm(everyone, cgate_v[...]), mm(everyone, cup_v[...])))
+    send_pieces(5 * batch, (lead + 1) * batch)
     extra[...] = narrow(mm(hidden, cdown_v[...])).reshape(size, 1, tokens, width)
     start_reduce(groups, True)
-    for k in range(1, close):
+    for k in range(1, relay * batch):
+        if k != CLOSE_PLACE:
+            pass_on(k)
+    for fetch in fetches[3:]:
+        fetch.wait()
+
+    def near_arrive():
+        k = CLOSE_PLACE
         for j in range(half):
             exchange(k, j, True).wait_recv()
         near_copy(k).start()
         for j in range(1, half):
             forward(k, j).start()
-    for k in range(close, relay * batch):
-        pass_on(k)
-    for fetch in fetches[3:]:
-        fetch.wait()
+
+    if batch > 1:
+        near_arrive()
 
     piece_rows = size * batch * block
     row = lax.broadcasted_iota(jnp.int32, (piece_rows, gate_v.shape[2]), 0)
@@ -858,7 +904,7 @@
             for b in range(batch):
                 action(base * batch + b)
 
-        @pl.when(t + lead < steps)
+        @pl.when((t > 0) & (t + lead < steps))
         def _():
             def action(k):
                 exchange(k).wait_recv()
@@ -868,7 +914,12 @@
 
         @pl.when(t + relay < steps)
         def _():
-            each(t + relay, pass_on)
+            def relay_piece(k):
+                @pl.when(k != CLOSE_PLACE)
+                def _():
+                    pass_on(k)
+
+            each(t + relay, relay_piece)
 
         @pl.when(t < steps)
         def _():
@@ -892,14 +943,20 @@
             )
             each(t, start_reduce)
 
+        if batch == 1:
+
+            @pl.when(t == NEAR_TURN)
+            def _():
+                near_arrive()
+
         @pl.when((t >= 1) & (t <= steps))
         def _():
             def action(k):
-                @pl.when(k < close)
+                @pl.when((k == 0) | (k == CLOSE_PLACE))
                 def _():
                     finish_close(k)
 
-                @pl.when(k >= close)
+                @pl.when((k > 0) & (k != CLOSE_PLACE))
                 def _():
                     add_pair(k)
 
@@ -912,7 +969,7 @@
         @pl.when(t >= 2)
         def _():
             def action(k):
-                @pl.when(k >= close)
+                @pl.when((k > 0) & (k != CLOSE_PLACE))
                 def _():
                     stage[k] = narrow(total_of(k))
                     back(k).start()
@@ -924,8 +981,9 @@
     lax.fori_loop(0, steps + 2, turn, 0)
 
     shared = total_of(groups, True)
-    for k in range(close, groups):
-        back(k, 0, flip(own, k, groups)).wait_recv()
+    for k in range(1, groups):
+        if k != CLOSE_PLACE:
+            back(k, 0, flip(own, piece(k, groups), groups)).wait_recv()
     out[...] = narrow(
         residual_scale * stream[...].astype(jnp.float32)
         + weighed(mix[...], returned[...])
@@ -933,11 +991,13 @@
     )
 
     for k in range(1, groups):
-        for j in range(half if k < close else 1):
-            exchange(k, j, k < close).wait_send()
+        direct = k == CLOSE_PLACE
+        for j in range(half if direct else 1):
+            exchange(k, j, direct).wait_send()
             back(k, j).wait_send()
     for k in range(groups + 1):
         whole = k == groups
+        direct = k in (0, CLOSE_PLACE)
         for j in range(half):
             reduce_near(k, j, whole).wait_send()
         if k > 0:
@@ -945,7 +1005,7 @@
         for j in range(1, half):
             if k > 0:
                 forward(k, j, whole).wait_send()
-            if k >= close:
+            if not direct:
                 far_copy(k, j, whole).wait_send()
                 reduce_far(k, j, whole).wait_send()
     for j in range(1, half):
@@ -1031,7 +1091,6 @@
     lanes = 2 * HEAD
     pairs = width_in // lanes
     chunks = rows // BLOCK_SPAN
-    close = min(CLOSE, groups)
     half = sides // 2
     f32, b16 = jnp.float32, jnp.bfloat16
     dma = pltpu.SemaphoreType.DMA
@@ -1074,10 +1133,10 @@
     moe_scratch = (
         [
             vmem((groups, block, width), b16),
-            vmem((close, half, block, width), b16),
+            vmem((half, block, width), b16),
             vmem((half - 1, groups, block, width), b16),
             vmem((half - 1, slots, tokens), f32),
-            vmem((half - 1, close, block, width), b16),
+            vmem((half - 1, block, width), b16),
             vmem((sides, groups, block, width), b16),
             vmem((sides, tokens, width), b16),
             vmem((sides, groups, block, width), b16),

time: 96.9 us -> 92.9 us (0.959)
  Pallas kernels: 95 us -> 91 us
    pallas_call x1, Pallas kernels: 95 us -> 91 us  [layer(): pl.pallas_call(lambda *refs: layer_kernel(groups, sides, block, capacity,...]
where the time goes in v4:
time: 92.9 us; the launch traced here: 92.7 us
  Pallas kernels  91 us (98%)
  local copies, waits for them, and re-layouts  1.67 us (2%)
    pallas_call x1, Pallas kernels, layer(): pl.pallas_call(lambda *refs: layer_kernel(groups, sides, block, capacity,...  91 us

profile of v4, /device:TPU:0, one launch (start us, length us, event | category | flops | bytes accessed | tf_op | source)
XLA Modules:
  0.0 92.7 jit_solution(8328240178221788207)
XLA Ops:
  0.0 91.0 %shard_map.181 = bf16[64,2048]{1,0:T(8,128)(2,1)} custom-call(bf16[256,512]{1,0:T(8,128)(2,1)} %refs_0_.1, bf16[256,512]{1,0:T(8,128)(2,1)} %refs_1_.1, bf16[256,512]{1,0:T(8,128)(2,1)} %refs_2_.1, bf16[256,512]{1,0:T(8,128)(2,1)} %refs_3_.1, bf16[8,256]{1,0:T(8,128)(2,1)} %bitcast.9, f32[8,256]{1,0:T(8,128)} %bitcast.7, s32[1,256]{1,0:T(1,128)} %bitcast.12, ...), custom_call_target="tpu_custom_call" | custom-call | tf_op jit(solution)/shard_map/pallas_call | solution.py:1160
  91.1 1.7 %copy.21 = bf16[64,2048]{1,0:T(8,128)(2,1)} copy(bf16[64,2048]{1,0:T(8,128)(2,1)} %shard_map.181) | data formatting | bytes 524288
